TPU v7x, 256 devices: a whole 4x4x8 slice. The times are simulated.
256 devices in a mesh: ep: 64 (over z, y, core), tp: 4 (over x).
Axes of the slice: x: 4, y: 4, z: 8, core: 2. Of those that a mesh axis runs over, the one named last changes fastest.
Arguments:
- tokens: bfloat16 [1536, 1024], P('ep'), may hold values from -6 to 6
- mixer_gain: float32 [1024], replicated, may hold values from 0.1 to 1.9
- gate_weight: bfloat16 [1024, 1024], P(None, 'tp'), may hold values from -0.1875 to 0.1875
- inner_weight: bfloat16 [1024, 1024], P(None, 'tp'), may hold values from -0.1875 to 0.1875
- state_weight: bfloat16 [2, 1024, 512], P(None, None, 'tp'), may hold values from -0.1875 to 0.1875
- step_weight: bfloat16 [1024, 16], P(None, 'tp'), may hold values from -0.1875 to 0.1875
- step_bias: float32 [16], P('tp'), may hold values from -4 to 0.5
- decay_log: float32 [16], P('tp'), may hold values from 0 to 2.8
- skip_scale: float32 [16], P('tp'), may hold values from 0.5 to 1.5
- inner_kernel: float32 [4, 1024], P(None, 'tp'), may hold values from -3 to 3
- state_kernel: float32 [4, 2, 512], P(None, None, 'tp'), may hold values from -3 to 3
- inner_window: bfloat16 [1536, 3, 1024], P('ep', None, 'tp'), may hold values from -6 to 6
- state_window: bfloat16 [1536, 3, 2, 512], P('ep', None, None, 'tp'), may hold values from -6 to 6
- recurrent_state: float32 [1536, 16, 64, 128], P('ep', 'tp'), may hold values from -2.4 to 2.4
- group_gain: float32 [1024], P('tp'), may hold values from 0.1 to 1.9
- output_weight: bfloat16 [1024, 1024], P('tp'), may hold values from -0.1875 to 0.1875
- channel_gain: float32 [1024], replicated, may hold values from 0.1 to 1.9
- routes: int32 [1536, 2], P('ep'), may hold values from 0 to 63, all different within a row; in each aligned block of 24 rows (0 to 23, 24 to 47, ...) at most 2 rows name the same one
- route_weights: float32 [1536, 2], P('ep'), may hold values from 0.2 to 1
- expert_gate: bfloat16 [64, 1024, 2816], P('ep', None, 'tp'), may hold values from -0.1875 to 0.1875
- expert_up: bfloat16 [64, 1024, 2816], P('ep', None, 'tp'), may hold values from -0.1875 to 0.1875
- expert_down: bfloat16 [64, 2816, 1024], P('ep', 'tp'), may hold values from -0.109375 to 0.109375
- dense_gate: bfloat16 [1024, 2816], P('tp', 'ep'), may hold values from -0.1875 to 0.1875
- dense_up: bfloat16 [1024, 2816], P('tp', 'ep'), may hold values from -0.1875 to 0.1875
- dense_down: bfloat16 [2816, 1024], P('ep', 'tp'), may hold values from -0.109375 to 0.109375
- dense_scale: float32 [1024], P('tp'), may hold values from 0.3 to 1.5
Outputs:
- new_tokens: bfloat16 [1536, 1024], P('ep', 'tp')
- new_state: float32 [1536, 16, 64, 128], P('ep', 'tp')
- new_inner_window: bfloat16 [1536, 3, 1024], P('ep', None, 'tp')
- new_state_window: bfloat16 [1536, 3, 2, 512], P('ep', None, None, 'tp')
Inputs may be any that keep to these rules, and one draw needn't show every extreme that they name: `routes`: each row names 2 different experts. Within the rows of one device (aligned blocks of 24 rows) no expert is named by more than 2 rows, and in some block an expert is named by exactly 2 rows.
All inputs are finite; a program needn't handle non-finite values.
Results may differ from a plain program's by a relative error of at most 0.014.
Values may be sent and summed in bfloat16 or wider, within the bound.
A program may use at most 64 MiB of HBM per device.

v0:
```python
import jax
import jax.numpy as jnp
from jax import lax
from jax.sharding import PartitionSpec as P

HEADS = 16
GROUPS = 4
HEAD_DIM = 64
STATE_DIM = 128


eps = 1e-06


def copy_for_each(x, axis):
    peers = lax.axis_size(axis)
    return lax.all_to_all(jnp.broadcast_to(x[None], (peers, *x.shape)), axis, 0, 0, tiled=True)


def of_everyone(x, axis):
    return copy_for_each(x, axis).astype(jnp.float32).sum(axis=0)


def turned_gather(arrays, axis, dims):
    turned = [jnp.moveaxis(a, dim, 0) for a, dim in zip(arrays, dims)]
    widths = [t[0].size for t in turned]
    both = jnp.concatenate([t.reshape(-1, w) for t, w in zip(turned, widths)], axis=1)
    result = lax.all_gather(both, axis, axis=0, tiled=True)
    blocks = jnp.split(result, [sum(widths[:k]) for k in range(1, len(widths))], axis=1)
    return tuple(
        (
            jnp.moveaxis(b.reshape(-1, *t.shape[1:]), 0, dim)
            for b, t, dim in zip(blocks, turned, dims)
        )
    )


def split_up(x, dim, peers):
    before, after = (x.shape[:dim], x.shape[dim + 1 :])
    return jnp.moveaxis(x.reshape(*before, peers, -1, *after), dim, 0)


def sent_and_summed(x, axis, dim):
    peers = lax.axis_size(axis)
    blocks = lax.all_to_all(split_up(x, dim, peers), axis, 0, 0, tiled=True)
    return jnp.sum(blocks.astype(jnp.float32), axis=0)


def rms_scale(values, norm_gain):
    squares = jnp.mean(values * values, axis=-1, keepdims=True)
    return values * lax.rsqrt(squares + eps) * norm_gain


def local(
    tokens,
    mixer_gain,
    gate_weight,
    inner_weight,
    state_weight,
    step_weight,
    step_bias,
    decay_log,
    skip_scale,
    inner_kernel,
    state_kernel,
    inner_window,
    state_window,
    recurrent_state,
    group_gain,
    output_weight,
    channel_gain,
    routes,
    route_weights,
    expert_gate,
    expert_up,
    expert_down,
    dense_gate,
    dense_up,
    dense_down,
    dense_scale,
):
    f32 = jnp.float32
    bf16 = jnp.bfloat16
    seq_count = tokens.shape[0]
    residual = tokens.astype(f32)
    normed = rms_scale(residual, mixer_gain).astype(bf16)
    gate_pre = jnp.dot(normed, gate_weight, preferred_element_type=f32)
    inner_pre = jnp.dot(normed, inner_weight, preferred_element_type=f32).astype(bf16)
    state_pre = jnp.stack(
        [
            jnp.dot(normed, state_weight[0], preferred_element_type=f32),
            jnp.dot(normed, state_weight[1], preferred_element_type=f32),
        ],
        axis=1,
    ).astype(bf16)
    step_raw = jnp.dot(normed, step_weight, preferred_element_type=f32)
    inner_ctx = jnp.concatenate([inner_window, inner_pre[:, None, :]], axis=1)
    inner_conv = jax.nn.silu(jnp.sum(inner_ctx.astype(f32) * inner_kernel[None], axis=1))
    state_ctx = jnp.concatenate([state_window, state_pre[:, None]], axis=1)
    state_conv = jax.nn.silu(jnp.sum(state_ctx.astype(f32) * state_kernel[None], axis=1))
    per_group = HEADS // GROUPS
    local_groups = state_conv.shape[-1] // STATE_DIM
    step_size = jax.nn.softplus(step_raw + step_bias)
    decay_rate = jnp.exp(-step_size * jnp.exp(decay_log))
    shaped = (seq_count, local_groups, per_group)
    inner_heads = inner_conv.reshape(seq_count, local_groups, per_group, HEAD_DIM)
    in_vector = state_conv[:, 0].reshape(seq_count, local_groups, STATE_DIM)
    out_vector = state_conv[:, 1].reshape(seq_count, local_groups, STATE_DIM)
    old_state = recurrent_state.reshape(seq_count, local_groups, per_group, HEAD_DIM, STATE_DIM)
    written = (step_size.reshape(shaped)[..., None] * inner_heads)[..., None] * in_vector[
        :, :, None, None, :
    ]
    new_state = old_state * decay_rate.reshape(shaped)[..., None, None] + written
    mixed_out = jnp.einsum(
        "sgrpn,sgn->sgrp", new_state, out_vector, precision=lax.Precision.HIGHEST
    )
    mixed_out = (
        mixed_out + skip_scale.reshape(local_groups, per_group)[None, :, :, None] * inner_heads
    )
    gated_out = mixed_out.reshape(seq_count, -1) * jax.nn.silu(gate_pre)
    grouped = rms_scale(gated_out.reshape(seq_count, local_groups, -1), 1.0).reshape(seq_count, -1)
    mixer_rows = (grouped * group_gain).astype(bf16)
    partial_value = jnp.dot(mixer_rows, output_weight, preferred_element_type=f32)
    residual = residual + of_everyone(partial_value.astype(jnp.bfloat16), "tp").astype(jnp.float32)
    ffn_rows = rms_scale(residual, channel_gain).astype(bf16)
    local_width = dense_gate.shape[0]
    tp_index = lax.axis_index("tp")
    own_columns = lax.dynamic_slice_in_dim(ffn_rows, tp_index * local_width, local_width, 1)
    residual_columns = lax.dynamic_slice_in_dim(residual, tp_index * local_width, local_width, 1)
    gate_whole, up_whole, down_whole = turned_gather(
        (dense_gate, dense_up, dense_down), "ep", (1, 1, 0)
    )
    gate_up = jnp.stack(
        [
            jnp.dot(own_columns, gate_whole, preferred_element_type=f32),
            jnp.dot(own_columns, up_whole, preferred_element_type=f32),
        ],
        axis=0,
    )
    gate_up = of_everyone(gate_up.astype(jnp.bfloat16), "tp").astype(jnp.float32)
    hidden_rows = (jax.nn.silu(gate_up[0]) * gate_up[1]).astype(bf16)
    dense_out = jnp.dot(hidden_rows, down_whole, preferred_element_type=f32)
    topk_count = routes.shape[1]
    local_experts = expert_gate.shape[0]
    expert_count = local_experts * lax.axis_size("ep")
    capacity = max(2, seq_count * topk_count * 3 // (2 * expert_count))
    flat_routes = routes.reshape(-1)
    onehot = (flat_routes[:, None] == jnp.arange(expert_count, dtype=jnp.int32)[None, :]).astype(
        jnp.int32
    )
    rank_before = jnp.cumsum(onehot, axis=0) - onehot
    slot_index = jnp.sum(rank_before * onehot, axis=1)
    target = flat_routes * capacity + slot_index
    placing = jnp.arange(expert_count * capacity, dtype=jnp.int32)[:, None] == target[None, :]
    selection = jnp.any(
        placing.reshape(expert_count * capacity, seq_count, topk_count), axis=2
    ).astype(bf16)
    outgoing = jnp.dot(selection, ffn_rows, preferred_element_type=f32).astype(bf16)
    outgoing = outgoing.reshape(expert_count, capacity, -1)
    arrived = lax.all_to_all(outgoing, "ep", split_axis=0, concat_axis=0, tiled=True)
    sources = arrived.shape[0] // local_experts
    items = arrived.shape[1]
    grouped_in = arrived.reshape(sources, local_experts, items, arrived.shape[2])
    gate_act = jnp.einsum("seid,edf->seif", grouped_in, expert_gate, preferred_element_type=f32)
    up_act = jnp.einsum("seid,edf->seif", grouped_in, expert_up, preferred_element_type=f32)
    activated = (jax.nn.silu(gate_act) * up_act).astype(bf16)
    partial_out = jnp.einsum("seif,efd->seid", activated, expert_down, preferred_element_type=f32)
    partial_out = partial_out.reshape(arrived.shape[0], items, -1)
    processed = sent_and_summed(partial_out.astype(jnp.bfloat16), "tp", 2).astype(bf16)
    returned = lax.all_to_all(processed, "ep", split_axis=0, concat_axis=0, tiled=True)
    returned_rows = returned.reshape(expert_count * capacity, -1)
    picked = jnp.einsum(
        "ms,md->sd", placing.astype(bf16), returned_rows, preferred_element_type=f32
    )
    expert_out = jnp.sum(
        picked.reshape(seq_count, topk_count, -1) * route_weights[:, :, None], axis=1
    )
    new_tokens = (residual_columns + expert_out + dense_scale * dense_out).astype(bf16)
    return (
        new_tokens,
        new_state.reshape(seq_count, -1, HEAD_DIM, STATE_DIM),
        inner_ctx[:, 1:],
        state_ctx[:, 1:],
    )


def solution(mesh):
    placed = (
        P("ep", None),
        P(),
        P(None, "tp"),
        P(None, "tp"),
        P(None, None, "tp"),
        P(None, "tp"),
        P("tp"),
        P("tp"),
        P("tp"),
        P(None, "tp"),
        P(None, None, "tp"),
        P("ep", None, "tp"),
        P("ep", None, None, "tp"),
        P("ep", "tp", None, None),
        P("tp"),
        P("tp", None),
        P(),
        P("ep", None),
        P("ep", None),
        P("ep", None, "tp"),
        P("ep", None, "tp"),
        P("ep", "tp", None),
        P("tp", "ep"),
        P("tp", "ep"),
        P("ep", "tp"),
        P("tp"),
    )
    return jax.shard_map(
        local,
        mesh=mesh,
        in_specs=placed,
        out_specs=(
            P("ep", "tp"),
            P("ep", "tp", None, None),
            P("ep", None, "tp"),
            P("ep", None, None, "tp"),
        ),
        check_vma=False,
    )
```

profile of v0, /device:TPU:1, one launch (start us, length us, event | category | flops | bytes accessed | tf_op | source)
XLA Modules:
  0.0 134.5 jit_solution(12523721000816451954)
XLA Ops:
  7.2 0.0 copy-start
  7.2 0.0 copy-start.3
  7.2 0.0 all-gather.3.cloned.1.call-start
  7.3 1.5 %maximum_bitcast_fusion = bf16[1,44,768]{2,1,0:T(8,128)(2,1)} fusion(bf16[44,256]{1,0:T(8,128)(2,1)} %param.50, bf16[44,256]{1,0:T(8,128)(2,1)} %bitcast.117, bf16[44,256]{1,0:T(8,128)(2,1)} %bitcast.118), kind=kLoop, calls=%fused_computation.67 | loop fusion | flops 202752 | bytes 135168
  8.8 0.0 all-gather.3.cloned.1.call-update
  8.8 0.7 exp.37
  9.5 0.9 fusion.65
  10.4 1.0 multiply_exponential_fusion
  11.5 0.1 copy.82
  11.6 0.1 copy.83
  11.7 1.3 fusion.43
  13.0 0.8 multiply_reduce_fusion.2
  13.8 0.1 reduce_sum.99
  13.9 1.2 fusion.44
  15.1 0.2 fusion.45
  15.4 0.1 multiply_reduce_fusion.1
  15.6 0.1 broadcast_multiply_fusion
  15.6 2.6 %multiply_add_fusion = f32[24,4,64,128]{3,2,1,0:T(8,128)S(1)} fusion(f32[24,4,64,128]{3,2,1,0:T(8,128)} %param.39, f32[24,128]{1,0:T(8,128)S(1)} %bitcast.116, f32[24,4,64]{2,1,0:T(4,128)S(1)} %broadcast_multiply_fusion, f32[24,4]{1,0:T(8,128)S(1)} %copy.82), kind=kLoop, calls=%fused_computation.4 | loop fusion | flops 2359296 | bytes 6328704 | tf_op jit(solution)/shard_map/add | solution.py:113
  18.2 0.0 copy-start.1
  18.3 7.4 %fusion.72 = f32[24,1,4,64]{3,1,2,0:T(1,128)S(1)} fusion(f32[24,4,64,128]{3,2,1,0:T(8,128)S(1)} %multiply_add_fusion, f32[24,2,128]{2,1,0:T(2,128)S(1)} %divide_multiply_fusion.1), kind=kOutput, calls=%fused_computation.87 | convolution fusion | flops 9437184 | bytes 3182592 | tf_op jit(solution)/shard_map/sgrpn,sgn->sgrp/dot_general | solution.py:114
  25.7 0.0 copy-start.15
  25.7 0.1 multiply_add_fusion.1
  25.8 0.1 reshape.236
  25.9 0.4 multiply_reduce_fusion.3
  26.3 0.2 convolution_convert_fusion.3
  26.5 0.7 broadcast_in_dim.7
  27.2 4.8 %all-to-all-start = ((bf16[4,24,1024]{2,1,0:T(8,128)(2,1)}), bf16[4,24,1024]{2,1,0:T(8,128)(2,1)S(1)}, u32[]{:S(2)}, u32[]{:S(2)}) async-start(bf16[4,24,1024]{2,1,0:T(8,128)(2,1)} %broadcast_in_dim.7), calls=%async_computation | async-start | bytes 393216 | tf_op jit(solution)/shard_map/all_to_all | solution.py:17
  32.0 0.1 copy.85
  32.1 0.1 reshape.237
  32.2 0.1 fusion.69
  32.3 0.1 reduce_window_sum.11
  32.4 0.2 select_reduce_fusion
  32.6 0.1 reduce_sum.104
  32.7 0.1 copy.86
  32.8 0.1 fusion.70
  32.8 4.4 %all-to-all-done = bf16[4,24,1024]{2,1,0:T(8,128)(2,1)S(1)} async-done(((bf16[4,24,1024]{2,1,0:T(8,128)(2,1)}), bf16[4,24,1024]{2,1,0:T(8,128)(2,1)S(1)}, u32[]{:S(2)}, u32[]{:S(2)}) %all-to-all-start) | async-done | bytes 196640 | tf_op jit(solution)/shard_map/all_to_all | solution.py:17
  37.3 0.1 multiply_reduce_fusion
  37.4 0.6 copy-done.6
  38.1 0.1 multiply_convert_fusion
  38.2 0.6 copy-done.7
  38.8 0.3 convolution_convert_fusion.2
  39.1 0.1 reshape.238
  39.2 26.6 %all_to_all.25 = bf16[64,2,1024]{2,1,0:T(2,128)(2,1)S(1)} all-to-all(bf16[64,2,1024]{2,1,0:T(2,128)(2,1)S(1)} %reshape.238), channel_id=1, replica_groups=mesh['ep'=64,'tp'=4] {'ep'}, dimensions={0} | all-to-all | bytes 524288 | tf_op jit(solution)/shard_map/all_to_all | solution.py:160
  65.7 0.6 fusion.12
  66.3 2.4 %fusion.27 = bf16[64,1,2,1024]{3,0,2,1:T(8,128)(2,1)S(1)} fusion(bf16[1,704,1024]{2,1,0:T(8,128)(2,1)S(1)} %copy-done, bf16[1,1024,704]{1,2,0:T(8,128)(2,1)} %param.46, f32[64,1,2,704]{3,0,2,1:T(8,128)S(1)} %fusion.12, bf16[64,2,1024]{2,1,0:T(2,128)(2,1)S(1)} %all_to_all.25), kind=kOutput, calls=%fused_computation.22 | convolution fusion | flops 369770496 | bytes 3768320 | tf_op jit(solution)/shard_map/seif,efd->seid/dot_general | solution.py:167
  68.8 0.2 convert_element_type.94
  69.0 0.7 copy.105
  69.7 3.4 %all-to-all-start.2 = ((bf16[4,64,2,256]{3,1,2,0:T(8,128)(2,1)}), bf16[4,64,2,256]{3,1,2,0:T(8,128)(2,1)S(1)}, u32[]{:S(2)}, u32[]{:S(2)}) async-start(bf16[4,64,2,256]{3,1,2,0:T(8,128)(2,1)} %bitcast.114), calls=%async_computation.2 | async-start | bytes 524288 | tf_op jit(solution)/shard_map/all_to_all | solution.py:45
  73.1 6.2 %all-to-all-done.2 = bf16[4,64,2,256]{3,1,2,0:T(8,128)(2,1)S(1)} async-done(((bf16[4,64,2,256]{3,1,2,0:T(8,128)(2,1)}), bf16[4,64,2,256]{3,1,2,0:T(8,128)(2,1)S(1)}, u32[]{:S(2)}, u32[]{:S(2)}) %all-to-all-start.2) | async-done | bytes 262176 | tf_op jit(solution)/shard_map/all_to_all | solution.py:45
  79.4 0.7 copy.91
  80.1 5.6 %all-to-all-start.3 = ((bf16[64,2,256]{2,1,0:T(2,128)(2,1)}), bf16[64,2,256]{2,1,0:T(2,128)(2,1)S(1)}, u32[]{:S(2)}, u32[]{:S(2)}) async-start(bf16[64,2,256]{2,1,0:T(2,128)(2,1)} %copy.91), calls=%async_computation.3 | async-start | bytes 131072 | tf_op jit(solution)/shard_map/all_to_all | solution.py:170
  85.7 8.6 %all-gather.3.cloned.1.call-done = bf16[64,44,768]{2,1,0:T(8,128)(2,1)} async-done(((bf16[1,44,768]{2,1,0:T(8,128)(2,1)}), bf16[64,44,768]{2,1,0:T(8,128)(2,1)}) %all-gather.3.cloned.1.call-update) | async-done | bytes 4325392 | tf_op jit(solution)/shard_map/all_gather | solution.py:28
  94.3 7.0 %reshape.245 = bf16[2816,768]{1,0:T(8,128)(2,1)} reshape(bf16[64,44,768]{2,1,0:T(8,128)(2,1)} %all-gather.3.cloned.1.call-done) | data formatting | bytes 8650752
  101.3 1.9 %fusion.1 = bf16[1,24,2816]{2,1,0:T(8,128)(2,1)S(1)} fusion(bf16[2816,768]{1,0:T(8,128)(2,1)} %reshape.245, bf16[24,1024]{1,0:T(8,128)(2,1)S(1)} %copy-done.8, s32[]{:T(128)S(6)} %select_n.9), kind=kOutput, calls=%fused_computation.3 | convolution fusion | flops 34670592 | bytes 1589252 | tf_op jit(solution)/shard_map/dot_general | solution.py:136
  103.2 1.9 %fusion = bf16[1,24,2816]{2,1,0:T(8,128)(2,1)S(1)} fusion(bf16[2816,768]{1,0:T(8,128)(2,1)} %reshape.245, bf16[24,1024]{1,0:T(8,128)(2,1)S(1)} %copy-done.8, s32[]{:T(128)S(6)} %select_n.9), kind=kOutput, calls=%fused_computation.2 | convolution fusion | flops 34670592 | bytes 1589252 | tf_op jit(solution)/shard_map/dot_general | solution.py:135
  105.1 1.0 broadcast_in_dim.8
  106.2 4.1 %all-to-all-start.4 = ((bf16[4,2,24,2816]{3,2,1,0:T(8,128)(2,1)}), bf16[4,2,24,2816]{3,2,1,0:T(8,128)(2,1)S(1)}, u32[]{:S(2)}, u32[]{:S(2)}) async-start(bf16[4,2,24,2816]{3,2,1,0:T(8,128)(2,1)} %broadcast_in_dim.8), calls=%async_computation.4 | async-start | bytes 2162688 | tf_op jit(solution)/shard_map/all_to_all | solution.py:17
  110.2 0.6 slice.38
  110.9 0.1 iota_compare_fusion.2
  111.0 0.6 fusion.68
  111.7 0.1 fusion.33
  111.7 13.5 %all-to-all-done.4 = bf16[4,2,24,2816]{3,2,1,0:T(8,128)(2,1)S(1)} async-done(((bf16[4,2,24,2816]{3,2,1,0:T(8,128)(2,1)}), bf16[4,2,24,2816]{3,2,1,0:T(8,128)(2,1)S(1)}, u32[]{:S(2)}, u32[]{:S(2)}) %all-to-all-start.4) | async-done | bytes 1081376 | tf_op jit(solution)/shard_map/all_to_all | solution.py:17
  125.2 0.1 convert_reduce_fusion
  125.4 2.3 %fusion.40 = bf16[24,256]{1,0:T(8,128)(2,1)} fusion(bf16[2816,768]{1,0:T(8,128)(2,1)} %reshape.245, f32[2,24,2816]{2,1,0:T(8,128)S(1)} %convert_reduce_fusion, f32[24,256]{1,0:T(8,128)S(1)} %fusion.33, f32[24,1024]{1,0:T(8,128)} %copy-done.6, s32[]{:T(128)S(6)} %select_n.9, f32[256]{0:T(256)S(1)} %copy-done.23), kind=kOutput, calls=%fused_computation.29 | convolution fusion | flops 35033088 | bytes 2044932 | tf_op jit(solution)/shard_map/dot_general | solution.py:142
  (58 shorter events, 0.4 us)
Async XLA Ops:
  7.2 59.2 %copy-start = (bf16[1,704,1024]{2,1,0:T(8,128)(2,1)S(1)}, bf16[1,704,1024]{2,1,0:T(8,128)(2,1)}, u32[]{:S(2)}) copy-start(bf16[1,704,1024]{2,1,0:T(8,128)(2,1)} %param.47) | copy-start | bytes 4325380
  7.2 7.9 %copy-start.3 = (bf16[24,1024]{1,0:T(8,128)(2,1)S(1)}, bf16[24,1024]{1,0:T(8,128)(2,1)}, u32[]{:S(2)}) copy-start(bf16[24,1024]{1,0:T(8,128)(2,1)} %param.26) | copy-start | bytes 147460
  7.2 7.9 %copy-start.13 = (f32[1024]{0:T(1024)S(1)}, f32[1024]{0:T(1024)}, u32[]{:S(2)}) copy-start(f32[1024]{0:T(1024)} %param.27) | copy-start | bytes 12292
  7.2 7.9 %copy-start.21 = (bf16[2,1024,128]{2,1,0:T(8,128)(2,1)S(1)}, bf16[2,1024,128]{2,1,0:T(8,128)(2,1)}, u32[]{:S(2)}) copy-start(bf16[2,1024,128]{2,1,0:T(8,128)(2,1)} %param.30) | copy-start | bytes 1572868
  7.2 8.1 %copy-start.12 = (bf16[24,3,2,128]{3,2,1,0:T(2,128)(2,1)S(1)}, bf16[24,3,2,128]{3,2,1,0:T(2,128)(2,1)}, u32[]{:S(2)}) copy-start(bf16[24,3,2,128]{3,2,1,0:T(2,128)(2,1)} %param.38) | copy-start | bytes 110596
  7.2 8.2 %copy-start.14 = (f32[4,2,128]{2,1,0:T(2,128)S(1)}, f32[4,2,128]{2,1,0:T(2,128)}, u32[]{:S(2)}) copy-start(f32[4,2,128]{2,1,0:T(2,128)} %param.36) | copy-start | bytes 12292
  7.2 87.0 %all-gather.3.cloned.1.call-start = ((), (), s32[]{:S(2)}) async-start(), calls=%async_computation.5 | async-start | bytes 4792320 | tf_op jit(solution)/shard_map/all_gather | solution.py:28
  15.4 2.8 %copy-start.9 = (bf16[24,4,2,128]{3,2,1,0:T(2,128)(2,1)}, bf16[24,4,2,128]{3,2,1,0:T(2,128)(2,1)S(1)}, u32[]{:S(2)}) copy-start(bf16[24,4,2,128]{3,2,1,0:T(2,128)(2,1)S(1)} %copy_dynamic-update-slice_fusion) | copy-start | bytes 147460
  18.2 7.5 %copy-start.1 = (f32[24,4,64,128]{3,2,1,0:T(8,128)}, f32[24,4,64,128]{3,2,1,0:T(8,128)S(1)}, u32[]{:S(2)}) copy-start(f32[24,4,64,128]{3,2,1,0:T(8,128)S(1)} %multiply_add_fusion) | copy-start | bytes 9437188
  18.2 7.5 %copy-start.20 = (f32[4]{0:T(128)S(1)}, f32[4]{0:T(128)}, u32[]{:S(2)}) copy-start(f32[4]{0:T(128)} %param.34) | copy-start | bytes 52
  18.3 7.6 %copy-start.4 = (bf16[1024,256]{1,0:T(8,128)(2,1)S(1)}, bf16[1024,256]{1,0:T(8,128)(2,1)}, u32[]{:S(2)}) copy-start(bf16[1024,256]{1,0:T(8,128)(2,1)} %param.28) | copy-start | bytes 1572868
  18.3 8.0 %copy-start.5 = (bf16[256,1024]{1,0:T(8,128)(2,1)S(1)}, bf16[256,1024]{1,0:T(8,128)(2,1)}, u32[]{:S(2)}) copy-start(bf16[256,1024]{1,0:T(8,128)(2,1)} %param.41) | copy-start | bytes 1572868
  18.3 8.0 %copy-start.19 = (f32[256]{0:T(256)S(1)}, f32[256]{0:T(256)}, u32[]{:S(2)}) copy-start(f32[256]{0:T(256)} %param.40) | copy-start | bytes 3076
  25.7 6.4 %copy-start.16 = (s32[24,2]{0,1:T(2,128)S(1)}, s32[24,2]{0,1:T(2,128)}, u32[]{:S(2)}) copy-start(s32[24,2]{0,1:T(2,128)} %param.43) | copy-start | bytes 580
  25.7 12.4 %copy-start.15 = (f32[1024]{0:T(1024)S(1)}, f32[1024]{0:T(1024)}, u32[]{:S(2)}) copy-start(f32[1024]{0:T(1024)} %param.42) | copy-start | bytes 12292
  26.5 39.2 %copy-start.2 = (bf16[1,1024,704]{1,2,0:T(8,128)(2,1)S(1)}, bf16[1,1024,704]{1,2,0:T(8,128)(2,1)}, u32[]{:S(2)}) copy-start(bf16[1,1024,704]{1,2,0:T(8,128)(2,1)} %param.45) | copy-start | bytes 4325380
  27.2 10.1 %all-to-all-start = ((bf16[4,24,1024]{2,1,0:T(8,128)(2,1)}), bf16[4,24,1024]{2,1,0:T(8,128)(2,1)S(1)}, u32[]{:S(2)}, u32[]{:S(2)}) async-start(bf16[4,24,1024]{2,1,0:T(8,128)(2,1)} %broadcast_in_dim.7), calls=%async_computation | async-start | bytes 393216 | tf_op jit(solution)/shard_map/all_to_all | solution.py:17
  32.6 5.6 %copy-start.17 = (s32[48]{0:T(128)}, s32[48]{0:T(128)S(1)}, u32[]{:S(2)}) copy-start(s32[48]{0:T(128)S(1)} %select_reduce_fusion) | copy-start | bytes 580
  37.4 0.6 copy-start.6
  38.2 0.6 copy-start.7
  69.7 9.6 %all-to-all-start.2 = ((bf16[4,64,2,256]{3,1,2,0:T(8,128)(2,1)}), bf16[4,64,2,256]{3,1,2,0:T(8,128)(2,1)S(1)}, u32[]{:S(2)}, u32[]{:S(2)}) async-start(bf16[4,64,2,256]{3,1,2,0:T(8,128)(2,1)} %bitcast.114), calls=%async_computation.2 | async-start | bytes 524288 | tf_op jit(solution)/shard_map/all_to_all | solution.py:45
  80.1 25.0 %all-to-all-start.3 = ((bf16[64,2,256]{2,1,0:T(2,128)(2,1)}), bf16[64,2,256]{2,1,0:T(2,128)(2,1)S(1)}, u32[]{:S(2)}, u32[]{:S(2)}) async-start(bf16[64,2,256]{2,1,0:T(2,128)(2,1)} %copy.91), calls=%async_computation.3 | async-start | bytes 131072 | tf_op jit(solution)/shard_map/all_to_all | solution.py:170
  85.7 15.6 %copy-start.8 = (bf16[24,1024]{1,0:T(8,128)(2,1)S(1)}, bf16[24,1024]{1,0:T(8,128)(2,1)}, u32[]{:S(2)}) copy-start(bf16[24,1024]{1,0:T(8,128)(2,1)} %copy-done.7) | copy-start | bytes 147460
  105.1 5.1 %copy-start.10 = (bf16[24,4,2,128]{3,2,1,0:T(2,128)(2,1)S(1)}, bf16[24,4,2,128]{3,2,1,0:T(2,128)(2,1)}, u32[]{:S(2)}) copy-start(bf16[24,4,2,128]{3,2,1,0:T(2,128)(2,1)} %copy-done.9) | copy-start | bytes 147460
  106.2 4.7 %copy-start.18 = (s32[48]{0:T(128)S(1)}, s32[48]{0:T(128)}, u32[]{:S(2)}) copy-start(s32[48]{0:T(128)} %copy-done.17) | copy-start | bytes 580
  106.2 4.8 %copy-start.11 = (bf16[24,3,256]{2,0,1:T(8,128)(2,1)S(1)}, bf16[24,3,256]{2,0,1:T(8,128)(2,1)}, u32[]{:S(2)}) copy-start(bf16[24,3,256]{2,0,1:T(8,128)(2,1)} %param.37) | copy-start | bytes 110596
  106.2 5.5 %copy-start.22 = (f32[24,2]{0,1:T(2,128)S(1)}, f32[24,2]{0,1:T(2,128)}, u32[]{:S(2)}) copy-start(f32[24,2]{0,1:T(2,128)} %param.44) | copy-start | bytes 580
  106.2 19.1 %all-to-all-start.4 = ((bf16[4,2,24,2816]{3,2,1,0:T(8,128)(2,1)}), bf16[4,2,24,2816]{3,2,1,0:T(8,128)(2,1)S(1)}, u32[]{:S(2)}, u32[]{:S(2)}) async-start(bf16[4,2,24,2816]{3,2,1,0:T(8,128)(2,1)} %broadcast_in_dim.8), calls=%async_computation.4 | async-start | bytes 2162688 | tf_op jit(solution)/shard_map/all_to_all | solution.py:17
  110.2 15.1 %copy-start.23 = (f32[256]{0:T(256)S(1)}, f32[256]{0:T(256)}, u32[]{:S(2)}) copy-start(f32[256]{0:T(256)} %param.51) | copy-start | bytes 3076
Sparse Core Ops, SparseCore 0:
  10.8 83.4 all-gather.2
where the time goes:
time: 136 us; the launch traced here: 135 us
  waiting for transfers between devices  32.7 us (24%)
  blocking collectives  26.6 us (20%)
  matrix products  21.1 us (16%)
  starting transfers between devices  17.9 us (13%)
  between operations  14.5 us (11%)
  local copies, waits for them, and re-layouts  13.9 us (10%)
  other arithmetic  7.71 us (6%)
    all_to_all x1, blocking collectives, local(): lax.all_to_all(outgoing, 'ep', split_axis=0, concat_axis=0, tiled=True)  26.6 us
    all_to_all x2, waiting for transfers between devices, copy_for_each(): lax.all_to_all(jnp.broadcast_to(x[None], (peers, *x.shape)), axis, 0, 0,...  17.9 us
    all_to_all x2, starting transfers between devices, copy_for_each(): lax.all_to_all(jnp.broadcast_to(x[None], (peers, *x.shape)), axis, 0, 0,...  8.9 us
    all_gather x1, waiting for transfers between devices, turned_gather(): result = lax.all_gather(both, axis, axis=0, tiled=True)  8.58 us
    unnamed x51, local copies, waits for them, and re-layouts  8.49 us
    dot_general x1, matrix products, local(): jnp.einsum('sgrpn,sgn->sgrp', new_state, out_vector, precision=lax.Precis...  7.39 us
    all_to_all x1, waiting for transfers between devices, sent_and_summed(): blocks = lax.all_to_all(split_up(x, dim, peers), axis, 0, 0, tiled=True)  6.22 us
    all_to_all x1, starting transfers between devices, local(): lax.all_to_all(processed, 'ep', split_axis=0, concat_axis=0, tiled=True)  5.6 us
  transfers between devices with their start and end apart: 5, of which 4 were waited for; matrix products, arithmetic and copies ran while one was open for 27% of the time, Pallas kernels for 0%

commit v1 on v0

v1 whole, which is shorter than its diff:
```python
import functools

import jax
import jax.numpy as jnp
from jax import lax
from jax.experimental import pallas as pl
from jax.experimental.pallas import tpu as pltpu
from jax.sharding import PartitionSpec as P

MESH = pl.DeviceIdType.MESH
F32 = jnp.float32
BF16 = jnp.bfloat16
HEAD_DIM = 64
STATE_DIM = 128
NYC = 8
eps = 1e-06


def rms_scale(values, norm_gain):
    squares = jnp.mean(values * values, axis=-1, keepdims=True)
    return values * lax.rsqrt(squares + eps) * norm_gain


def dot(a, b):
    return jnp.dot(a, b, preferred_element_type=F32)


def mixer_kernel(
    tokens_ref,
    mixer_gain_ref,
    step_weight_ref,
    step_bias_ref,
    decay_log_ref,
    skip_ref,
    inner_kernel_ref,
    state_kernel_ref,
    inner_window_ref,
    state_window_ref,
    group_gain_ref,
    gate_weight_hbm,
    inner_weight_hbm,
    state_weight_hbm,
    output_weight_hbm,
    state_hbm,
    partial_ref,
    new_inner_ref,
    new_state_window_ref,
    new_state_hbm,
    gate_w,
    inner_w,
    state_w,
    output_w,
    state,
    in_sems,
    state_sems,
    out_sems,
):
    seqs = tokens_ref.shape[0]
    heads = state.shape[1]
    chunk = seqs // 4
    loads = [
        pltpu.make_async_copy(src, dst, in_sems.at[i])
        for i, (src, dst) in enumerate(
            [
                (inner_weight_hbm, inner_w),
                (state_weight_hbm, state_w),
                (gate_weight_hbm, gate_w),
                (output_weight_hbm, output_w),
            ]
        )
    ]
    for load in loads[:3]:
        load.start()
    state_loads = [
        pltpu.make_async_copy(
            state_hbm.at[pl.ds(c * chunk, chunk)], state.at[pl.ds(c * chunk, chunk)], state_sems.at[c]
        )
        for c in range(4)
    ]
    for load in state_loads:
        load.start()
    loads[3].start()

    residual = tokens_ref[...].astype(F32)
    normed = rms_scale(residual, mixer_gain_ref[...]).astype(BF16)
    step_raw = dot(normed, step_weight_ref[...])
    step_in = step_raw + step_bias_ref[...]
    step = jnp.maximum(step_in, 0.0) + jnp.log1p(jnp.exp(-jnp.abs(step_in)))
    decay = jnp.exp(-step * jnp.exp(decay_log_ref[...]))

    inner_window = inner_window_ref[...].astype(F32)
    loads[0].wait()
    inner_pre = dot(normed, inner_w[...]).astype(BF16).astype(F32)
    kern = inner_kernel_ref[...]
    conv = inner_pre * kern[3:4]
    for j in range(3):
        conv = conv + inner_window[:, j, :] * kern[j : j + 1]
    inner = jax.nn.silu(conv)
    new_inner_ref[...] = jnp.concatenate(
        [inner_window[:, 1:3, :], inner_pre[:, None, :]], axis=1
    ).astype(BF16)

    loads[1].wait()
    vectors = []
    pres = []
    for r in range(2):
        pre = dot(normed, state_w[r]).astype(BF16).astype(F32)
        conv = pre * state_kernel_ref[3, r : r + 1, :]
        for j in range(3):
            conv = conv + state_window_ref[:, j, r, :].astype(F32) * state_kernel_ref[j, r : r + 1, :]
        vectors.append(jax.nn.silu(conv))
        pres.append(pre)
    new_state_window_ref[:, 0:2] = state_window_ref[:, 1:3]
    new_state_window_ref[:, 2] = jnp.concatenate(
        [pres[0][:, None, :], pres[1][:, None, :]], axis=1
    ).astype(BF16)
    in_vector, out_vector = vectors

    loads[2].wait()
    gate_pre = dot(normed, gate_w[...])

    lane = lax.broadcasted_iota(jnp.int32, inner.shape, 1) // HEAD_DIM
    step_wide = jnp.broadcast_to(step[:, 0:1], inner.shape)
    skip_wide = jnp.broadcast_to(skip_ref[:, 0:1], inner.shape)
    for h in range(1, heads):
        step_wide = jnp.where(lane == h, step[:, h : h + 1], step_wide)
        skip_wide = jnp.where(lane == h, skip_ref[:, h : h + 1], skip_wide)
    written = jnp.transpose(step_wide * inner)

    columns = lax.broadcasted_iota(jnp.int32, (HEAD_DIM, STATE_DIM), 1)
    mixed = [jnp.zeros((HEAD_DIM, STATE_DIM), F32) for _ in range(heads)]
    stores = []
    for b in range(seqs):
        if b % chunk == 0:
            state_loads[b // chunk].wait()
        u = in_vector[b : b + 1, :]
        c = out_vector[b : b + 1, :]
        for h in range(heads):
            new = state[b, h] * decay[b : b + 1, h : h + 1] + (
                written[h * HEAD_DIM : (h + 1) * HEAD_DIM, b : b + 1] * u
            )
            state[b, h] = new
            read = jnp.sum(new * c, axis=1, keepdims=True)
            mixed[h] = jnp.where(columns == b, read, mixed[h])
        if b % chunk == chunk - 1:
            k = b // chunk
            store = pltpu.make_async_copy(
                state.at[pl.ds(k * chunk, chunk)], new_state_hbm.at[pl.ds(k * chunk, chunk)], out_sems.at[k]
            )
            store.start()
            stores.append(store)
    mixed_rows = jnp.transpose(jnp.concatenate(mixed, axis=0))[:seqs, :]
    mixed_rows = mixed_rows + skip_wide * inner
    gated = mixed_rows * jax.nn.silu(gate_pre)
    rows = (rms_scale(gated, 1.0) * group_gain_ref[...]).astype(BF16)
    loads[3].wait()
    partial_ref[...] = dot(rows, output_w[...]).astype(BF16)
    for store in stores:
        store.wait()


def ffn_kernel(
    n_ep,
    n_tp,
    partial_ref,
    tokens_ref,
    gain_ref,
    routes_ref,
    route_weights_ref,
    dense_gate_ref,
    dense_up_ref,
    dense_down_ref,
    dense_scale_ref,
    gate_hbm,
    up_hbm,
    down_hbm,
    out_ref,
    w_gate,
    w_up,
    w_down,
    parts,
    residual_ref,
    ffn_ref,
    gu,
    dn,
    dx,
    tall,
    going,
    came,
    xs,
    act,
    dz_going,
    dz_came,
    hid,
    moe_going,
    moe_came,
    tall_back,
    back_going,
    back_came,
    od_going,
    od_came,
    local_sems,
    send_sems,
    recv_sems,
):
    me = lax.axis_index("ep")
    t = lax.axis_index("tp")
    n_z = n_ep // NYC
    z = me // NYC
    yc = me % NYC
    seqs = tokens_ref.shape[0]
    width = out_ref.shape[1]
    slots = 2 * n_ep

    def across_tp(k):
        return (me, (t + k) % n_tp)

    def along_z(k):
        return (((z + k) % n_z) * NYC + yc, t)

    def within_z(k):
        return (z * NYC + (yc + k) % NYC, t)

    def along_ep(k):
        return ((me + k) % n_ep, t)

    def remote(src, dst, which, peer):
        return pltpu.make_async_remote_copy(
            src_ref=src,
            dst_ref=dst,
            send_sem=send_sems.at[which],
            recv_sem=recv_sems.at[which],
            device_id=peer,
            device_id_type=MESH,
        )

    def wait_in(ref, which):
        remote(ref, ref, which, across_tp(1)).wait_recv()

    def wait_out(ref, which):
        remote(ref, ref, which, across_tp(1)).wait_send()

    PART, GU, DN, DX, OUT, DZ, HID, MOE, BACK, OD = range(10)

    barrier = pltpu.get_barrier_semaphore()
    for k in range(1, n_tp):
        pl.semaphore_signal(barrier, inc=1, device_id=across_tp(k), device_id_type=MESH)

    def greet(k, carry):
        pl.semaphore_signal(barrier, inc=1, device_id=along_ep(k), device_id_type=MESH)
        return carry

    lax.fori_loop(1, n_ep, greet, 0)

    loads = [
        pltpu.make_async_copy(src.at[0], dst, local_sems.at[i])
        for i, (src, dst) in enumerate([(gate_hbm, w_gate), (up_hbm, w_up), (down_hbm, w_down)])
    ]
    for load in loads:
        load.start()

    units = dense_gate_ref.shape[1]
    gap = jnp.zeros((width, 64 - units), F32)
    gu[yc] = jnp.concatenate(
        [dense_gate_ref[...].astype(F32), gap, dense_up_ref[...].astype(F32), gap], axis=1
    ).astype(BF16)
    dn[yc] = jnp.concatenate(
        [dense_down_ref[...].astype(F32), jnp.zeros((64 - units, width), F32)], axis=0
    ).astype(BF16)
    parts[t] = partial_ref[...]

    expert = lax.broadcasted_iota(jnp.int32, (seqs, n_ep), 1)
    named = [(routes_ref[:, k : k + 1] == expert).astype(F32) for k in range(2)]
    earlier = (
        lax.broadcasted_iota(jnp.int32, (seqs, seqs), 0)
        > lax.broadcasted_iota(jnp.int32, (seqs, seqs), 1)
    ).astype(F32)
    before = dot(earlier, named[0] + named[1])
    place = lax.broadcasted_iota(jnp.int32, (seqs, slots), 1)
    chosen = []
    for k in range(2):
        slot = jnp.sum(before * named[k], axis=1, keepdims=True).astype(jnp.int32)
        chosen.append((place == routes_ref[:, k : k + 1] * 2 + slot).astype(F32))
    selection = jnp.transpose(chosen[0] + chosen[1]).astype(BF16)

    pl.semaphore_wait(barrier, n_tp - 1 + n_ep - 1)

    for k in range(1, n_tp):
        remote(partial_ref, parts.at[t], PART, across_tp(k)).start()

    def share_gate_up(k, carry):
        remote(gu.at[yc], gu.at[yc], GU, within_z(k)).start()
        return carry

    def share_down(k, carry):
        remote(dn.at[yc], dn.at[yc], DN, within_z(k)).start()
        return carry

    lax.fori_loop(1, NYC, share_gate_up, 0)
    lax.fori_loop(1, NYC, share_down, 0)

    wait_in(parts.at[pl.ds(0, n_tp - 1)], PART)
    total = parts[0].astype(F32)
    for k in range(1, n_tp):
        total = total + parts[k].astype(F32)
    residual = tokens_ref[...].astype(F32) + total
    residual_ref[...] = residual
    ffn = rms_scale(residual, gain_ref[...]).astype(BF16)
    ffn_ref[...] = ffn

    own = pl.ds(pl.multiple_of(t * width, width), width)
    dx[z] = ffn_ref[:, own]

    def share_tokens(k, carry):
        remote(dx.at[z], dx.at[z], DX, along_z(k)).start()
        return carry

    lax.fori_loop(1, n_z, share_tokens, 0)

    outgoing = dot(selection, ffn)
    lines = outgoing.shape[1] // 128
    for j in range(lines):
        tall[pl.ds(j, slots, stride=lines), :] = outgoing[:, j * 128 : (j + 1) * 128]
    going[...] = tall[...].reshape(going.shape).astype(BF16)

    def dispatch(k, carry):
        peer = along_ep(k)
        remote(going.at[peer[0]], came.at[me], OUT, peer).start()
        return carry

    lax.fori_loop(1, n_ep, dispatch, 0)
    came[me] = going[me]

    wait_in(gu.at[pl.ds(0, NYC - 1)], GU)
    wait_in(dx.at[pl.ds(0, n_z - 1)], DX)
    dense_rows = dx[...].reshape(n_z * seqs, width)
    for s in range(NYC):
        dz_going[:, :, s * 128 : (s + 1) * 128] = (
            dot(dense_rows, gu[s]).astype(BF16).reshape(n_tp, -1, 128)
        )
    for k in range(1, n_tp):
        peer = across_tp(k)
        remote(dz_going.at[peer[1]], dz_came.at[t], DZ, peer).start()
    dz_came[t] = dz_going[t]

    wait_in(came.at[pl.ds(0, n_ep - 1)], OUT)
    tall[...] = came[...].astype(F32).reshape(tall.shape)
    for j in range(lines):
        xs[:, j * 128 : (j + 1) * 128] = tall[pl.ds(j, slots, stride=lines), :].astype(BF16)
    loads[0].wait()
    loads[1].wait()
    rows = xs[...]
    act[...] = (jax.nn.silu(dot(rows, w_gate[...])) * dot(rows, w_up[...])).astype(BF16)
    loads[2].wait()
    for k in range(1, n_tp):
        peer = across_tp(k)
        columns = pl.ds(pl.multiple_of(peer[1] * width, width), width)
        moe_going[peer[1]] = dot(act[...], w_down[:, columns]).astype(BF16)
        remote(moe_going.at[peer[1]], moe_came.at[t], MOE, peer).start()
    moe_came[t] = dot(act[...], w_down[:, own]).astype(BF16)

    wait_in(dz_came.at[pl.ds(0, n_tp - 1)], DZ)
    low = lax.broadcasted_iota(jnp.int32, (dz_came.shape[1], 128), 1) < 64
    halves = []
    for s in range(NYC):
        block = dz_came[0, :, s * 128 : (s + 1) * 128].astype(F32)
        for k in range(1, n_tp):
            block = block + dz_came[k, :, s * 128 : (s + 1) * 128].astype(F32)
        up = pltpu.roll(block, 64, 1)
        halves.append(jax.nn.silu(block) * up)
    for s in range(NYC // 2):
        hid[t, :, s * 128 : (s + 1) * 128] = jnp.where(
            low, halves[2 * s], pltpu.roll(halves[2 * s + 1], 64, 1)
        ).astype(BF16)
    for k in range(1, n_tp):
        remote(hid.at[t], hid.at[t], HID, across_tp(k)).start()

    wait_in(moe_came.at[pl.ds(0, n_tp - 1)], MOE)
    rows_out = moe_came[0].astype(F32)
    for k in range(1, n_tp):
        rows_out = rows_out + moe_came[k].astype(F32)
    for j in range(width // 128):
        tall_back[pl.ds(j, slots, stride=4), :] = rows_out[:, j * 128 : (j + 1) * 128]
    back_going[...] = tall_back[...].reshape(back_going.shape).astype(BF16)

    def give_back(k, carry):
        peer = along_ep(k)
        remote(back_going.at[peer[0]], back_came.at[me], BACK, peer).start()
        return carry

    lax.fori_loop(1, n_ep, give_back, 0)
    back_came[me] = back_going[me]

    wait_in(dn.at[pl.ds(0, NYC - 1)], DN)
    wait_in(hid.at[pl.ds(0, n_tp - 1)], HID)
    dense_part = dot(
        hid[...].reshape(n_z * seqs, NYC * 64), dn[...].reshape(NYC * 64, width)
    )
    od_going[...] = dense_part.astype(BF16).reshape(od_going.shape)

    def share_out(k, carry):
        there = (z + k) % n_z
        remote(od_going.at[there], od_came.at[z], OD, along_z(k)).start()
        return carry

    lax.fori_loop(1, n_z, share_out, 0)
    od_came[z] = od_going[z]

    wait_in(od_came.at[pl.ds(0, n_z - 1)], OD)
    dense_out = od_came[0].astype(F32)
    for k in range(1, n_z):
        dense_out = dense_out + od_came[k].astype(F32)

    wait_in(back_came.at[pl.ds(0, n_ep - 1)], BACK)
    tall_back[...] = back_came[...].astype(F32).reshape(tall_back.shape)
    returned = [
        tall_back[pl.ds(j, slots, stride=4), :].astype(BF16) for j in range(width // 128)
    ]
    returned = jnp.concatenate(returned, axis=1)
    expert_out = jnp.zeros((seqs, width), F32)
    for k in range(2):
        expert_out = expert_out + route_weights_ref[:, k : k + 1] * dot(
            chosen[k].astype(BF16), returned
        )
    out_ref[...] = (
        residual_ref[:, own] + expert_out + dense_scale_ref[...] * dense_out
    ).astype(BF16)

    wait_out(parts.at[pl.ds(0, n_tp - 1)], PART)
    wait_out(gu.at[pl.ds(0, NYC - 1)], GU)
    wait_out(dn.at[pl.ds(0, NYC - 1)], DN)
    wait_out(dx.at[pl.ds(0, n_z - 1)], DX)
    wait_out(going.at[pl.ds(0, n_ep - 1)], OUT)
    wait_out(dz_going.at[pl.ds(0, n_tp - 1)], DZ)
    wait_out(hid.at[pl.ds(0, n_tp - 1)], HID)
    wait_out(moe_going.at[pl.ds(0, n_tp - 1)], MOE)
    wait_out(back_going.at[pl.ds(0, n_ep - 1)], BACK)
    wait_out(od_going.at[pl.ds(0, n_z - 1)], OD)


VMEM = pl.BlockSpec(memory_space=pltpu.VMEM)
ANY = pl.BlockSpec(memory_space=pl.ANY)


def local(
    n_ep,
    n_tp,
    tokens,
    mixer_gain,
    gate_weight,
    inner_weight,
    state_weight,
    step_weight,
    step_bias,
    decay_log,
    skip_scale,
    inner_kernel,
    state_kernel,
    inner_window,
    state_window,
    recurrent_state,
    group_gain,
    output_weight,
    channel_gain,
    routes,
    route_weights,
    expert_gate,
    expert_up,
    expert_down,
    dense_gate,
    dense_up,
    dense_down,
    dense_scale,
):
    seqs, model = tokens.shape
    width = dense_scale.shape[0]
    hidden = expert_gate.shape[2]
    n_z = n_ep // NYC
    slots = 2 * n_ep
    sds = jax.ShapeDtypeStruct
    partial, new_inner, new_window, new_state = pl.pallas_call(
        mixer_kernel,
        out_shape=(
            sds((seqs, model), BF16),
            sds(inner_window.shape, BF16),
            sds(state_window.shape, BF16),
            sds(recurrent_state.shape, F32),
        ),
        in_specs=[VMEM] * 11 + [ANY] * 5,
        out_specs=(VMEM, VMEM, VMEM, ANY),
        scratch_shapes=[
            pltpu.VMEM(gate_weight.shape, BF16),
            pltpu.VMEM(inner_weight.shape, BF16),
            pltpu.VMEM(state_weight.shape, BF16),
            pltpu.VMEM(output_weight.shape, BF16),
            pltpu.VMEM(recurrent_state.shape, F32),
            pltpu.SemaphoreType.DMA((4,)),
            pltpu.SemaphoreType.DMA((4,)),
            pltpu.SemaphoreType.DMA((4,)),
        ],
        name="mixer",
    )(
        tokens,
        mixer_gain[None],
        step_weight,
        step_bias[None],
        decay_log[None],
        skip_scale[None],
        inner_kernel,
        state_kernel,
        inner_window,
        state_window,
        group_gain[None],
        gate_weight,
        inner_weight,
        state_weight,
        output_weight,
        recurrent_state,
    )
    scratch = [
        pltpu.VMEM((model, hidden), BF16),
        pltpu.VMEM((model, hidden), BF16),
        pltpu.VMEM((hidden, model), BF16),
        pltpu.VMEM((n_tp, seqs, model), BF16),
        pltpu.VMEM((seqs, model), F32),
        pltpu.VMEM((seqs, model), BF16),
        pltpu.VMEM((NYC, width, 128), BF16),
        pltpu.VMEM((NYC, 64, width), BF16),
        pltpu.VMEM((n_z, seqs, width), BF16),
        pltpu.VMEM((slots * model // 128, 128), F32),
        pltpu.VMEM((n_ep, 2 * model // 128, 128), BF16),
        pltpu.VMEM((n_ep, 2 * model // 128, 128), BF16),
        pltpu.VMEM((slots, model), BF16),
        pltpu.VMEM((slots, hidden), BF16),
        pltpu.VMEM((n_tp, n_z * seqs // n_tp, NYC * 128), BF16),
        pltpu.VMEM((n_tp, n_z * seqs // n_tp, NYC * 128), BF16),
        pltpu.VMEM((n_tp, n_z * seqs // n_tp, NYC * 64), BF16),
        pltpu.VMEM((n_tp, slots, width), BF16),
        pltpu.VMEM((n_tp, slots, width), BF16),
        pltpu.VMEM((slots * 4, 128), F32),
        pltpu.VMEM((n_ep, 8, 128), BF16),
        pltpu.VMEM((n_ep, 8, 128), BF16),
        pltpu.VMEM((n_z, seqs, width), BF16),
        pltpu.VMEM((n_z, seqs, width), BF16),
        pltpu.SemaphoreType.DMA((3,)),
        pltpu.SemaphoreType.DMA((10,)),
        pltpu.SemaphoreType.DMA((10,)),
    ]
    new_tokens = pl.pallas_call(
        functools.partial(ffn_kernel, n_ep, n_tp),
        out_shape=sds((seqs, width), BF16),
        in_specs=[VMEM] * 9 + [ANY] * 3,
        out_specs=VMEM,
        scratch_shapes=scratch,
        compiler_params=pltpu.CompilerParams(collective_id=0, has_side_effects=True),
        name="ffn",
    )(
        partial,
        tokens,
        channel_gain[None],
        routes,
        route_weights,
        dense_gate,
        dense_up,
        dense_down,
        dense_scale[None],
        expert_gate,
        expert_up,
        expert_down,
    )
    return new_tokens, new_state, new_inner, new_window


def solution(mesh):
    placed = (
        P("ep", None),
        P(),
        P(None, "tp"),
        P(None, "tp"),
        P(None, None, "tp"),
        P(None, "tp"),
        P("tp"),
        P("tp"),
        P("tp"),
        P(None, "tp"),
        P(None, None, "tp"),
        P("ep", None, "tp"),
        P("ep", None, None, "tp"),
        P("ep", "tp", None, None),
        P("tp"),
        P("tp", None),
        P(),
        P("ep", None),
        P("ep", None),
        P("ep", None, "tp"),
        P("ep", None, "tp"),
        P("ep", "tp", None),
        P("tp", "ep"),
        P("tp", "ep"),
        P("ep", "tp"),
        P("tp"),
    )
    return jax.shard_map(
        functools.partial(local, mesh.shape["ep"], mesh.shape["tp"]),
        mesh=mesh,
        in_specs=placed,
        out_specs=(
            P("ep", "tp"),
            P("ep", "tp", None, None),
            P("ep", None, "tp"),
            P("ep", None, None, "tp"),
        ),
        check_vma=False,
    )
```

time: 136 us -> 73.8 us (0.54)
  Pallas kernels: 0 us -> 61.9 us
  waiting for transfers between devices: 32.7 us -> 0 us
  blocking collectives: 26.6 us -> 0 us
  matrix products: 21.1 us -> 0 us
  starting transfers between devices: 17.9 us -> 0 us
  between operations: 14.5 us -> 0.69 us
  other arithmetic: 7.71 us -> 0 us
  local copies, waits for them, and re-layouts: 13.9 us -> 10.9 us
    pallas_call x0 -> x2, Pallas kernels: none -> 61.9 us  [the longest x1 45.7 us: local(): pl.pallas_call(functools.partial(ffn_kernel, n_ep, n_tp), out_shape=sds((...]
    all_to_all x1 -> x0, blocking collectives: 26.6 us -> none  [local(): lax.all_to_all(outgoing, 'ep', split_axis=0, concat_axis=0, tiled=True)]
    all_to_all x4 -> x0, waiting for transfers between devices: 24.1 us -> none  [the longest x2 17.9 us: copy_for_each(): lax.all_to_all(jnp.broadcast_to(x[None], (peers, *x.shape)), axis, 0, 0,...]
    dot_general x14 -> x0, matrix products: 21.1 us -> none  [the longest x1 7.39 us: local(): jnp.einsum('sgrpn,sgn->sgrp', new_state, out_vector, precision=lax.Precis...]
    all_to_all x4 -> x0, starting transfers between devices: 17.9 us -> none  [the longest x2 8.9 us: copy_for_each(): lax.all_to_all(jnp.broadcast_to(x[None], (peers, *x.shape)), axis, 0, 0,...]
    all_gather x1 -> x0, waiting for transfers between devices: 8.58 us -> none  [turned_gather(): result = lax.all_gather(both, axis, axis=0, tiled=True)]
    add x4 -> x0, other arithmetic: 2.66 us -> none  [the longest x1 2.57 us: local(): old_state * decay_rate.reshape(shaped)[..., None, None] + written]
    unnamed x51 -> x24, local copies, waits for them, and re-layouts: 8.49 us -> 10.9 us
  transfers between devices with their start and end apart: 5 -> 0, of which waited for: 4 -> 0; matrix products, arithmetic and copies ran while one was open for 27% -> 0% of each run, Pallas kernels for 0% -> 0%
where the time goes in v1:
time: 73.8 us; the launch traced here: 73.5 us
  Pallas kernels  61.9 us (84%)
  local copies, waits for them, and re-layouts  10.9 us (15%)
    pallas_call x1, Pallas kernels, local(): pl.pallas_call(functools.partial(ffn_kernel, n_ep, n_tp), out_shape=sds((...  45.7 us
    pallas_call x1, Pallas kernels, local(): pl.pallas_call(mixer_kernel, out_shape=(sds((seqs, model), BF16), sds(inn...  16.2 us
    unnamed x24, local copies, waits for them, and re-layouts  10.9 us

profile of v1, /device:TPU:1, one launch (start us, length us, event | category | flops | bytes accessed | tf_op | source)
XLA Modules:
  0.0 73.5 jit_solution(15723627958232090078)
XLA Ops:
  0.6 1.6 %copy.30.step_weight_ref = bf16[1024,4]{1,0:T(8,128)(2,1)} copy(bf16[1024,4]{0,1:T(4,128)(2,1)} %param.31) | data formatting | bytes 16384 | tf_op args[5]
  2.2 1.4 %copy.31.inner_window_ref = bf16[24,3,256]{2,1,0:T(4,128)(2,1)} copy(bf16[24,3,256]{2,0,1:T(8,128)(2,1)} %param.37) | data formatting | bytes 73728 | tf_op args[11]
  3.6 0.0 copy-start
  3.6 16.2 %mixer.1 = (bf16[24,1024]{1,0:T(8,128)(2,1)}, bf16[24,3,256]{2,1,0:T(4,128)(2,1)}, bf16[24,3,2,128]{3,2,1,0:T(2,128)(2,1)}, f32[24,4,64,128]{3,2,1,0:T(8,128)}) custom-call(bf16[24,1024]{1,0:T(8,128)(2,1)} %tokens_ref.3, f32[1,1024]{1,0:T(1,128)} %bitcast.7, bf16[1024,4]{1,0:T(8,128)(2,1)} %copy.30.step_weight_ref, f32[1,4]{1,0:T(1,128)} %bitcast.11, ...), custom_call_target="tpu_custom_call" | custom-call | tf_op jit(solution)/shard_map/mixer/pallas_call | solution.py:481
  19.8 0.0 copy-start.1
  19.8 0.0 copy-done
  19.8 1.6 %copy.36.gate_hbm = bf16[1,1024,704]{2,1,0:T(8,128)(2,1)} copy(bf16[1,1024,704]{1,2,0:T(8,128)(2,1)S(1)} %copy-done) | data formatting | bytes 2883584 | tf_op args[19]
  21.4 0.0 copy-done.1
  21.4 0.0 copy-start.3
  21.4 0.0 copy-start.4
  21.4 0.0 copy-start.5
  21.4 0.0 copy-start.6
  21.4 1.6 %copy.37.up_hbm = bf16[1,1024,704]{2,1,0:T(8,128)(2,1)} copy(bf16[1,1024,704]{1,2,0:T(8,128)(2,1)S(1)} %copy-done.1) | data formatting | bytes 2883584 | tf_op args[20]
  23.0 0.0 copy-done.3
  23.0 0.7 copy.34.dense_gate_ref
  23.7 0.0 copy-done.4
  23.7 0.7 copy.35.dense_up_ref
  24.5 0.0 copy-done.5
  24.5 0.7 copy.32.routes_ref
  25.2 0.0 copy-done.6
  25.2 0.7 copy.33.route_weights_ref
  25.8 0.0 copy-start.2
  25.8 45.7 %ffn.1 = bf16[24,256]{1,0:T(8,128)(2,1)} custom-call(bf16[24,1024]{1,0:T(8,128)(2,1)} %get-tuple-element.8.partial_ref, bf16[24,1024]{1,0:T(8,128)(2,1)} %tokens_ref.3, f32[1,1024]{1,0:T(1,128)} %bitcast.8, s32[24,2]{1,0:T(8,128)} %copy.32.routes_ref, f32[24,2]{1,0:T(8,128)} %copy.33.route_weights_ref, bf16[256,44]{1,0:T(8,128)(2,1)} %copy.34.dense_gate_ref, ...), custom_call_target="tpu_custom_call" | custom-call | tf_op jit(solution)/shard_map/ffn/pallas_call | solution.py:549
  71.6 0.0 copy-done.2
  71.6 0.6 copy.38
  72.2 1.3 %copy.40 = bf16[24,256]{1,0:T(8,128)(2,1)} copy(bf16[24,256]{1,0:T(8,128)(2,1)} %ffn.1) | data formatting | bytes 24576
Async XLA Ops:
  3.6 16.2 %copy-start = (bf16[1,1024,704]{1,2,0:T(8,128)(2,1)S(1)}, bf16[1,1024,704]{1,2,0:T(8,128)(2,1)}, u32[]{:S(2)}) copy-start(bf16[1,1024,704]{1,2,0:T(8,128)(2,1)} %param.45) | copy-start | bytes 4325380
  19.8 1.6 %copy-start.1 = (bf16[1,1024,704]{1,2,0:T(8,128)(2,1)S(1)}, bf16[1,1024,704]{1,2,0:T(8,128)(2,1)}, u32[]{:S(2)}) copy-start(bf16[1,1024,704]{1,2,0:T(8,128)(2,1)} %param.46) | copy-start | bytes 4325380
  21.4 1.6 %copy-start.3 = (bf16[256,44]{0,1:T(8,128)(2,1)S(1)}, bf16[256,44]{0,1:T(8,128)(2,1)}, u32[]{:S(2)}) copy-start(bf16[256,44]{0,1:T(8,128)(2,1)} %param.48) | copy-start | bytes 67588
  21.4 2.3 %copy-start.4 = (bf16[256,44]{0,1:T(8,128)(2,1)S(1)}, bf16[256,44]{0,1:T(8,128)(2,1)}, u32[]{:S(2)}) copy-start(bf16[256,44]{0,1:T(8,128)(2,1)} %param.49) | copy-start | bytes 67588
  21.4 3.1 %copy-start.5 = (s32[24,2]{0,1:T(2,128)S(1)}, s32[24,2]{0,1:T(2,128)}, u32[]{:S(2)}) copy-start(s32[24,2]{0,1:T(2,128)} %param.43) | copy-start | bytes 580
  21.4 3.7 %copy-start.6 = (f32[24,2]{0,1:T(2,128)S(1)}, f32[24,2]{0,1:T(2,128)}, u32[]{:S(2)}) copy-start(f32[24,2]{0,1:T(2,128)} %param.44) | copy-start | bytes 580
  25.8 45.7 %copy-start.2 = (bf16[24,3,256]{2,1,0:T(4,128)(2,1)S(1)}, bf16[24,3,256]{2,1,0:T(4,128)(2,1)}, u32[]{:S(2)}) copy-start(bf16[24,3,256]{2,1,0:T(4,128)(2,1)} %get-tuple-element.14) | copy-start | bytes 110596

commit v2 on v1

--- a/solution.py
+++ b/solution.py
@@ -13,6 +13,7 @@
 HEAD_DIM = 64
 STATE_DIM = 128
 NYC = 8
+UNITS = 48
 eps = 1e-06
 
 
@@ -23,6 +24,15 @@
 
 def dot(a, b):
     return jnp.dot(a, b, preferred_element_type=F32)
+
+
+def two_terms(v):
+    high = v.astype(BF16).astype(F32)
+    return high, (v - high).astype(BF16).astype(F32)
+
+
+def dot_rows(a, b):
+    return lax.dot_general(a, b, (((1,), (1,)), ((), ())), preferred_element_type=F32)
 
 
 def mixer_kernel(
@@ -51,6 +61,8 @@
     state_w,
     output_w,
     state,
+    decay_rows,
+    read,
     in_sems,
     state_sems,
     out_sems,
@@ -83,22 +95,20 @@
 
     residual = tokens_ref[...].astype(F32)
     normed = rms_scale(residual, mixer_gain_ref[...]).astype(BF16)
-    step_raw = dot(normed, step_weight_ref[...])
+    step_raw = dot_rows(normed, step_weight_ref[...])
     step_in = step_raw + step_bias_ref[...]
     step = jnp.maximum(step_in, 0.0) + jnp.log1p(jnp.exp(-jnp.abs(step_in)))
     decay = jnp.exp(-step * jnp.exp(decay_log_ref[...]))
 
-    inner_window = inner_window_ref[...].astype(F32)
     loads[0].wait()
     inner_pre = dot(normed, inner_w[...]).astype(BF16).astype(F32)
     kern = inner_kernel_ref[...]
     conv = inner_pre * kern[3:4]
     for j in range(3):
-        conv = conv + inner_window[:, j, :] * kern[j : j + 1]
+        conv = conv + inner_window_ref[j].astype(F32) * kern[j : j + 1]
     inner = jax.nn.silu(conv)
-    new_inner_ref[...] = jnp.concatenate(
-        [inner_window[:, 1:3, :], inner_pre[:, None, :]], axis=1
-    ).astype(BF16)
+    new_inner_ref[0:2] = inner_window_ref[1:3]
+    new_inner_ref[2] = inner_pre.astype(BF16)
 
     loads[1].wait()
     vectors = []
@@ -125,31 +135,53 @@
     for h in range(1, heads):
         step_wide = jnp.where(lane == h, step[:, h : h + 1], step_wide)
         skip_wide = jnp.where(lane == h, skip_ref[:, h : h + 1], skip_wide)
-    written = jnp.transpose(step_wide * inner)
-
-    columns = lax.broadcasted_iota(jnp.int32, (HEAD_DIM, STATE_DIM), 1)
-    mixed = [jnp.zeros((HEAD_DIM, STATE_DIM), F32) for _ in range(heads)]
+    for h in range(heads):
+        decay_rows[:, h * STATE_DIM : (h + 1) * STATE_DIM] = jnp.broadcast_to(
+            decay[:, h : h + 1], (seqs, STATE_DIM)
+        )
+    spare = jnp.zeros((32 - seqs, inner.shape[1]), F32)
+    high, low = two_terms(jnp.concatenate([step_wide * inner, spare], axis=0))
+    written = jnp.transpose(
+        jnp.concatenate([high, high, low, jnp.zeros_like(low)], axis=0)
+    ).astype(BF16)
+    spare = spare[:, :STATE_DIM]
+    high, low = two_terms(jnp.concatenate([in_vector, spare], axis=0))
+    inputs = jnp.concatenate([high, low, high, jnp.zeros_like(low)], axis=0)
+    owner = lax.broadcasted_iota(jnp.int32, inputs.shape, 0) % 32
+    high, low = two_terms(jnp.concatenate([out_vector, spare], axis=0))
+    reader = jnp.concatenate([high, low, jnp.zeros((64, STATE_DIM), F32)], axis=0).astype(BF16)
+    reader = jnp.concatenate([reader, reader], axis=1)
+    column = lax.broadcasted_iota(jnp.int32, (heads * HEAD_DIM, STATE_DIM), 1) % 32
+
     stores = []
-    for b in range(seqs):
-        if b % chunk == 0:
-            state_loads[b // chunk].wait()
-        u = in_vector[b : b + 1, :]
-        c = out_vector[b : b + 1, :]
-        for h in range(heads):
-            new = state[b, h] * decay[b : b + 1, h : h + 1] + (
-                written[h * HEAD_DIM : (h + 1) * HEAD_DIM, b : b + 1] * u
-            )
-            state[b, h] = new
-            read = jnp.sum(new * c, axis=1, keepdims=True)
-            mixed[h] = jnp.where(columns == b, read, mixed[h])
-        if b % chunk == chunk - 1:
-            k = b // chunk
-            store = pltpu.make_async_copy(
-                state.at[pl.ds(k * chunk, chunk)], new_state_hbm.at[pl.ds(k * chunk, chunk)], out_sems.at[k]
-            )
-            store.start()
-            stores.append(store)
-    mixed_rows = jnp.transpose(jnp.concatenate(mixed, axis=0))[:seqs, :]
+    for k in range(4):
+        state_loads[k].wait()
+
+        def update(i, carry):
+            b = k * chunk + i
+            added = dot(written, jnp.where(owner == b, inputs, 0.0).astype(BF16))
+            rates = decay_rows[pl.ds(b, 1), :]
+            news = []
+            for h in range(heads):
+                new = state[b, h] * rates[:, h * STATE_DIM : (h + 1) * STATE_DIM] + (
+                    added[h * HEAD_DIM : (h + 1) * HEAD_DIM]
+                )
+                state[b, h] = new
+                news.append(new)
+            new = jnp.concatenate(news, axis=0)
+            high = new.astype(BF16)
+            both = jnp.concatenate([high, (new - high.astype(F32)).astype(BF16)], axis=1)
+            read[...] = jnp.where(column == b, dot_rows(both, reader), read[...])
+            return carry
+
+        lax.fori_loop(0, chunk, update, 0, unroll=True)
+        store = pltpu.make_async_copy(
+            state.at[pl.ds(k * chunk, chunk)], new_state_hbm.at[pl.ds(k * chunk, chunk)], out_sems.at[k]
+        )
+        store.start()
+        stores.append(store)
+    mixed = jnp.transpose(read[...])
+    mixed_rows = mixed[:seqs] + mixed[32 : 32 + seqs]
     mixed_rows = mixed_rows + skip_wide * inner
     gated = mixed_rows * jax.nn.silu(gate_pre)
     rows = (rms_scale(gated, 1.0) * group_gain_ref[...]).astype(BF16)
@@ -181,9 +213,9 @@
     parts,
     residual_ref,
     ffn_ref,
-    gu,
-    dn,
+    dw,
     dx,
+    combine_ref,
     tall,
     going,
     came,
@@ -213,16 +245,23 @@
     slots = 2 * n_ep
 
     def across_tp(k):
-        return (me, (t + k) % n_tp)
+        return (me, lax.rem(t + k, n_tp))
 
     def along_z(k):
-        return (((z + k) % n_z) * NYC + yc, t)
+        return (lax.rem(z + k, n_z) * NYC + yc, t)
 
     def within_z(k):
-        return (z * NYC + (yc + k) % NYC, t)
-
-    def along_ep(k):
-        return ((me + k) % n_ep, t)
+        return (z * NYC + lax.rem(yc + k, NYC), t)
+
+    def along_ep(kz, k):
+        return (lax.rem(z + kz, n_z) * NYC + lax.rem(yc + k, NYC), t)
+
+    steps = sorted(range(n_z), key=lambda kz: -min(kz, n_z - kz))
+
+    def to_all(send):
+        for kz in steps:
+            for k in range(0 if kz else 1, NYC):
+                send(along_ep(kz, k))
 
     def remote(src, dst, which, peer):
         return pltpu.make_async_remote_copy(
@@ -240,17 +279,15 @@
     def wait_out(ref, which):
         remote(ref, ref, which, across_tp(1)).wait_send()
 
-    PART, GU, DN, DX, OUT, DZ, HID, MOE, BACK, OD = range(10)
+    PART, DW, DW2, DX, OUT, DZ, HID, MOE, BACK, OD = range(10)
 
     barrier = pltpu.get_barrier_semaphore()
     for k in range(1, n_tp):
         pl.semaphore_signal(barrier, inc=1, device_id=across_tp(k), device_id_type=MESH)
 
-    def greet(k, carry):
-        pl.semaphore_signal(barrier, inc=1, device_id=along_ep(k), device_id_type=MESH)
-        return carry
-
-    lax.fori_loop(1, n_ep, greet, 0)
+    to_all(
+        lambda peer: pl.semaphore_signal(barrier, inc=1, device_id=peer, device_id_type=MESH)
+    )
 
     loads = [
         pltpu.make_async_copy(src.at[0], dst, local_sems.at[i])
@@ -259,45 +296,38 @@
     for load in loads:
         load.start()
 
-    units = dense_gate_ref.shape[1]
-    gap = jnp.zeros((width, 64 - units), F32)
-    gu[yc] = jnp.concatenate(
-        [dense_gate_ref[...].astype(F32), gap, dense_up_ref[...].astype(F32), gap], axis=1
-    ).astype(BF16)
-    dn[yc] = jnp.concatenate(
-        [dense_down_ref[...].astype(F32), jnp.zeros((64 - units, width), F32)], axis=0
-    ).astype(BF16)
+    units = dense_gate_ref.shape[0]
+    gap = jnp.zeros((UNITS - units, width), F32)
+    for i, ref in enumerate((dense_gate_ref, dense_up_ref, dense_down_ref)):
+        dw[yc, i * UNITS : (i + 1) * UNITS] = jnp.concatenate(
+            [ref[...].astype(F32), gap], axis=0
+        ).astype(BF16)
     parts[t] = partial_ref[...]
 
-    expert = lax.broadcasted_iota(jnp.int32, (seqs, n_ep), 1)
-    named = [(routes_ref[:, k : k + 1] == expert).astype(F32) for k in range(2)]
+    expert = lax.broadcasted_iota(jnp.int32, (n_ep, seqs), 0)
+    named = [(routes_ref[k : k + 1, :] == expert).astype(F32) for k in range(2)]
     earlier = (
         lax.broadcasted_iota(jnp.int32, (seqs, seqs), 0)
-        > lax.broadcasted_iota(jnp.int32, (seqs, seqs), 1)
+        < lax.broadcasted_iota(jnp.int32, (seqs, seqs), 1)
     ).astype(F32)
-    before = dot(earlier, named[0] + named[1])
-    place = lax.broadcasted_iota(jnp.int32, (seqs, slots), 1)
+    before = dot(named[0] + named[1], earlier)
+    place = lax.broadcasted_iota(jnp.int32, (slots, seqs), 0)
     chosen = []
     for k in range(2):
-        slot = jnp.sum(before * named[k], axis=1, keepdims=True).astype(jnp.int32)
-        chosen.append((place == routes_ref[:, k : k + 1] * 2 + slot).astype(F32))
-    selection = jnp.transpose(chosen[0] + chosen[1]).astype(BF16)
+        slot = jnp.sum(before * named[k], axis=0, keepdims=True).astype(jnp.int32)
+        chosen.append((place == routes_ref[k : k + 1, :] * 2 + slot).astype(F32))
+    selection = (chosen[0] + chosen[1]).astype(BF16)
+    combine_ref[...] = jnp.transpose(
+        chosen[0] * route_weights_ref[0:1, :] + chosen[1] * route_weights_ref[1:2, :]
+    )
 
     pl.semaphore_wait(barrier, n_tp - 1 + n_ep - 1)
 
     for k in range(1, n_tp):
         remote(partial_ref, parts.at[t], PART, across_tp(k)).start()
 
-    def share_gate_up(k, carry):
-        remote(gu.at[yc], gu.at[yc], GU, within_z(k)).start()
-        return carry
-
-    def share_down(k, carry):
-        remote(dn.at[yc], dn.at[yc], DN, within_z(k)).start()
-        return carry
-
-    lax.fori_loop(1, NYC, share_gate_up, 0)
-    lax.fori_loop(1, NYC, share_down, 0)
+    for k in range(2, NYC, 2):
+        remote(dw.at[yc], dw.at[yc], DW, within_z(k)).start()
 
     wait_in(parts.at[pl.ds(0, n_tp - 1)], PART)
     total = parts[0].astype(F32)
@@ -311,11 +341,8 @@
     own = pl.ds(pl.multiple_of(t * width, width), width)
     dx[z] = ffn_ref[:, own]
 
-    def share_tokens(k, carry):
+    for k in steps[:-1]:
         remote(dx.at[z], dx.at[z], DX, along_z(k)).start()
-        return carry
-
-    lax.fori_loop(1, n_z, share_tokens, 0)
 
     outgoing = dot(selection, ffn)
     lines = outgoing.shape[1] // 128
@@ -323,20 +350,21 @@
         tall[pl.ds(j, slots, stride=lines), :] = outgoing[:, j * 128 : (j + 1) * 128]
     going[...] = tall[...].reshape(going.shape).astype(BF16)
 
-    def dispatch(k, carry):
-        peer = along_ep(k)
-        remote(going.at[peer[0]], came.at[me], OUT, peer).start()
-        return carry
-
-    lax.fori_loop(1, n_ep, dispatch, 0)
+    to_all(lambda peer: remote(going.at[peer[0]], came.at[me], OUT, peer).start())
     came[me] = going[me]
 
-    wait_in(gu.at[pl.ds(0, NYC - 1)], GU)
+    wait_in(dw.at[pl.ds(0, NYC // 2 - 1)], DW)
+    sibling = (z * NYC + yc + 1 - 2 * lax.rem(yc, 2), t)
+    for k in range(0, NYC, 2):
+        held = lax.rem(yc + k, NYC)
+        remote(dw.at[held], dw.at[held], DW2, sibling).start()
+    wait_in(dw.at[pl.ds(0, NYC // 2)], DW2)
     wait_in(dx.at[pl.ds(0, n_z - 1)], DX)
     dense_rows = dx[...].reshape(n_z * seqs, width)
-    for s in range(NYC):
-        dz_going[:, :, s * 128 : (s + 1) * 128] = (
-            dot(dense_rows, gu[s]).astype(BF16).reshape(n_tp, -1, 128)
+    for i in range(2):
+        weights = dw[:, i * UNITS : (i + 1) * UNITS].reshape(NYC * UNITS, width)
+        dz_going[:, :, i * NYC * UNITS : (i + 1) * NYC * UNITS] = (
+            dot_rows(dense_rows, weights).astype(BF16).reshape(n_tp, -1, NYC * UNITS)
         )
     for k in range(1, n_tp):
         peer = across_tp(k)
@@ -350,7 +378,7 @@
     loads[0].wait()
     loads[1].wait()
     rows = xs[...]
-    act[...] = (jax.nn.silu(dot(rows, w_gate[...])) * dot(rows, w_up[...])).astype(BF16)
+    act[...] = (jax.nn.silu(dot_rows(rows, w_gate[...])) * dot_rows(rows, w_up[...])).astype(BF16)
     loads[2].wait()
     for k in range(1, n_tp):
         peer = across_tp(k)
@@ -360,18 +388,12 @@
     moe_came[t] = dot(act[...], w_down[:, own]).astype(BF16)
 
     wait_in(dz_came.at[pl.ds(0, n_tp - 1)], DZ)
-    low = lax.broadcasted_iota(jnp.int32, (dz_came.shape[1], 128), 1) < 64
-    halves = []
-    for s in range(NYC):
-        block = dz_came[0, :, s * 128 : (s + 1) * 128].astype(F32)
-        for k in range(1, n_tp):
-            block = block + dz_came[k, :, s * 128 : (s + 1) * 128].astype(F32)
-        up = pltpu.roll(block, 64, 1)
-        halves.append(jax.nn.silu(block) * up)
-    for s in range(NYC // 2):
-        hid[t, :, s * 128 : (s + 1) * 128] = jnp.where(
-            low, halves[2 * s], pltpu.roll(halves[2 * s + 1], 64, 1)
-        ).astype(BF16)
+    gate_up = dz_came[0].astype(F32)
+    for k in range(1, n_tp):
+        gate_up = gate_up + dz_came[k].astype(F32)
+    hid[t] = (
+        jax.nn.silu(gate_up[:, : NYC * UNITS]) * gate_up[:, NYC * UNITS :]
+    ).astype(BF16)
     for k in range(1, n_tp):
         remote(hid.at[t], hid.at[t], HID, across_tp(k)).start()
 
@@ -383,27 +405,19 @@
         tall_back[pl.ds(j, slots, stride=4), :] = rows_out[:, j * 128 : (j + 1) * 128]
     back_going[...] = tall_back[...].reshape(back_going.shape).astype(BF16)
 
-    def give_back(k, carry):
-        peer = along_ep(k)
-        remote(back_going.at[peer[0]], back_came.at[me], BACK, peer).start()
-        return carry
-
-    lax.fori_loop(1, n_ep, give_back, 0)
+    to_all(lambda peer: remote(back_going.at[peer[0]], back_came.at[me], BACK, peer).start())
     back_came[me] = back_going[me]
 
-    wait_in(dn.at[pl.ds(0, NYC - 1)], DN)
     wait_in(hid.at[pl.ds(0, n_tp - 1)], HID)
     dense_part = dot(
-        hid[...].reshape(n_z * seqs, NYC * 64), dn[...].reshape(NYC * 64, width)
+        hid[...].reshape(n_z * seqs, NYC * UNITS),
+        dw[:, 2 * UNITS : 3 * UNITS].reshape(NYC * UNITS, width),
     )
     od_going[...] = dense_part.astype(BF16).reshape(od_going.shape)
 
-    def share_out(k, carry):
-        there = (z + k) % n_z
+    for k in steps[:-1]:
+        there = lax.rem(z + k, n_z)
         remote(od_going.at[there], od_came.at[z], OD, along_z(k)).start()
-        return carry
-
-    lax.fori_loop(1, n_z, share_out, 0)
     od_came[z] = od_going[z]
 
     wait_in(od_came.at[pl.ds(0, n_z - 1)], OD)
@@ -416,19 +430,15 @@
     returned = [
         tall_back[pl.ds(j, slots, stride=4), :].astype(BF16) for j in range(width // 128)
     ]
-    returned = jnp.concatenate(returned, axis=1)
-    expert_out = jnp.zeros((seqs, width), F32)
-    for k in range(2):
-        expert_out = expert_out + route_weights_ref[:, k : k + 1] * dot(
-            chosen[k].astype(BF16), returned
-        )
+    returned = jnp.concatenate(returned, axis=1).astype(F32)
+    expert_out = jnp.dot(combine_ref[...], returned, precision=lax.Precision.HIGHEST)
     out_ref[...] = (
         residual_ref[:, own] + expert_out + dense_scale_ref[...] * dense_out
     ).astype(BF16)
 
     wait_out(parts.at[pl.ds(0, n_tp - 1)], PART)
-    wait_out(gu.at[pl.ds(0, NYC - 1)], GU)
-    wait_out(dn.at[pl.ds(0, NYC - 1)], DN)
+    wait_out(dw.at[pl.ds(0, NYC // 2 - 1)], DW)
+    wait_out(dw.at[pl.ds(0, NYC // 2)], DW2)
     wait_out(dx.at[pl.ds(0, n_z - 1)], DX)
     wait_out(going.at[pl.ds(0, n_ep - 1)], OUT)
     wait_out(dz_going.at[pl.ds(0, n_tp - 1)], DZ)
@@ -482,7 +492,7 @@
         mixer_kernel,
         out_shape=(
             sds((seqs, model), BF16),
-            sds(inner_window.shape, BF16),
+            sds((3, seqs, width), BF16),
             sds(state_window.shape, BF16),
             sds(recurrent_state.shape, F32),
         ),
@@ -494,6 +504,8 @@
             pltpu.VMEM(state_weight.shape, BF16),
             pltpu.VMEM(output_weight.shape, BF16),
             pltpu.VMEM(recurrent_state.shape, F32),
+            pltpu.VMEM((seqs, step_bias.shape[0] * STATE_DIM), F32),
+            pltpu.VMEM((width, STATE_DIM), F32),
             pltpu.SemaphoreType.DMA((4,)),
             pltpu.SemaphoreType.DMA((4,)),
             pltpu.SemaphoreType.DMA((4,)),
@@ -502,13 +514,13 @@
     )(
         tokens,
         mixer_gain[None],
-        step_weight,
+        step_weight.T,
         step_bias[None],
         decay_log[None],
         skip_scale[None],
         inner_kernel,
         state_kernel,
-        inner_window,
+        jnp.swapaxes(inner_window, 0, 1),
         state_window,
         group_gain[None],
         gate_weight,
@@ -518,23 +530,23 @@
         recurrent_state,
     )
     scratch = [
-        pltpu.VMEM((model, hidden), BF16),
-        pltpu.VMEM((model, hidden), BF16),
+        pltpu.VMEM((hidden, model), BF16),
+        pltpu.VMEM((hidden, model), BF16),
         pltpu.VMEM((hidden, model), BF16),
         pltpu.VMEM((n_tp, seqs, model), BF16),
         pltpu.VMEM((seqs, model), F32),
         pltpu.VMEM((seqs, model), BF16),
-        pltpu.VMEM((NYC, width, 128), BF16),
-        pltpu.VMEM((NYC, 64, width), BF16),
+        pltpu.VMEM((NYC, 3 * UNITS, width), BF16),
         pltpu.VMEM((n_z, seqs, width), BF16),
+        pltpu.VMEM((seqs, slots), F32),
         pltpu.VMEM((slots * model // 128, 128), F32),
         pltpu.VMEM((n_ep, 2 * model // 128, 128), BF16),
         pltpu.VMEM((n_ep, 2 * model // 128, 128), BF16),
         pltpu.VMEM((slots, model), BF16),
         pltpu.VMEM((slots, hidden), BF16),
-        pltpu.VMEM((n_tp, n_z * seqs // n_tp, NYC * 128), BF16),
-        pltpu.VMEM((n_tp, n_z * seqs // n_tp, NYC * 128), BF16),
-        pltpu.VMEM((n_tp, n_z * seqs // n_tp, NYC * 64), BF16),
+        pltpu.VMEM((n_tp, n_z * seqs // n_tp, 2 * NYC * UNITS), BF16),
+        pltpu.VMEM((n_tp, n_z * seqs // n_tp, 2 * NYC * UNITS), BF16),
+        pltpu.VMEM((n_tp, n_z * seqs // n_tp, NYC * UNITS), BF16),
         pltpu.VMEM((n_tp, slots, width), BF16),
         pltpu.VMEM((n_tp, slots, width), BF16),
         pltpu.VMEM((slots * 4, 128), F32),
@@ -558,17 +570,17 @@
         partial,
         tokens,
         channel_gain[None],
-        routes,
-        route_weights,
-        dense_gate,
-        dense_up,
+        routes.T,
+        route_weights.T,
+        dense_gate.T,
+        dense_up.T,
         dense_down,
         dense_scale[None],
-        expert_gate,
-        expert_up,
+        jnp.swapaxes(expert_gate, 1, 2),
+        jnp.swapaxes(expert_up, 1, 2),
         expert_down,
     )
-    return new_tokens, new_state, new_inner, new_window
+    return new_tokens, new_state, jnp.swapaxes(new_inner, 0, 1), new_window
 
 
 def solution(mesh):

time: 73.8 us -> 53.8 us (0.73)
  Pallas kernels: 61.9 us -> 51.6 us
  local copies, waits for them, and re-layouts: 10.9 us -> 1.31 us
    unnamed x24 -> x1, local copies, waits for them, and re-layouts: 10.9 us -> 1.31 us
    pallas_call x1, Pallas kernels: 16.2 us -> 7.65 us  [local(): pl.pallas_call(mixer_kernel, out_shape=(sds((seqs, model), BF16), sds((3,...]
    pallas_call x1, Pallas kernels: 45.7 us -> 43.9 us  [local(): pl.pallas_call(functools.partial(ffn_kernel, n_ep, n_tp), out_shape=sds((...]
where the time goes in v2:
time: 53.8 us; the launch traced here: 53.5 us
  Pallas kernels  51.6 us (96%)
  local copies, waits for them, and re-layouts  1.31 us (2%)
  between operations  0.65 us (1%)
    pallas_call x1, Pallas kernels, local(): pl.pallas_call(functools.partial(ffn_kernel, n_ep, n_tp), out_shape=sds((...  43.9 us
    pallas_call x1, Pallas kernels, local(): pl.pallas_call(mixer_kernel, out_shape=(sds((seqs, model), BF16), sds((3,...  7.65 us
    unnamed x1, local copies, waits for them, and re-layouts  1.31 us

profile of v2, /device:TPU:1, one launch (start us, length us, event | category | flops | bytes accessed | tf_op | source)
XLA Modules:
  0.0 53.5 jit_solution(11428364488116350326)
XLA Ops:
  0.6 7.6 %mixer.1 = (bf16[24,1024]{1,0:T(8,128)(2,1)}, bf16[3,24,256]{2,1,0:T(8,128)(2,1)}, bf16[24,3,2,128]{3,2,1,0:T(2,128)(2,1)}, f32[24,4,64,128]{3,2,1,0:T(8,128)}) custom-call(bf16[24,1024]{1,0:T(8,128)(2,1)} %tokens_ref.3, f32[1,1024]{1,0:T(1,128)} %bitcast.23, bf16[4,1024]{1,0:T(4,128)(2,1)} %bitcast.21, f32[1,4]{1,0:T(1,128)} %bitcast.28, f32[1,4]{1,0:T(1,128)} %bitcast.29, ...), custom_call_target="tpu_custom_call" | custom-call | tf_op jit(solution)/shard_map/mixer/pallas_call | solution.py:491
  8.3 43.9 %ffn.1 = bf16[24,256]{1,0:T(8,128)(2,1)} custom-call(bf16[24,1024]{1,0:T(8,128)(2,1)} %get-tuple-element.8.partial_ref, bf16[24,1024]{1,0:T(8,128)(2,1)} %tokens_ref.3, f32[1,1024]{1,0:T(1,128)} %bitcast.22, s32[2,24]{1,0:T(2,128)} %bitcast.25, f32[2,24]{1,0:T(2,128)} %bitcast.26, bf16[44,256]{1,0:T(8,128)(2,1)} %bitcast.19, bf16[44,256]{1,0:T(8,128)(2,1)} %bitcast.20, ...), custom_call_target="tpu_custom_call" | custom-call | tf_op jit(solution)/shard_map/ffn/pallas_call | solution.py:561
  52.2 1.3 %copy.31 = bf16[24,256]{1,0:T(8,128)(2,1)} copy(bf16[24,256]{1,0:T(8,128)(2,1)} %ffn.1) | data formatting | bytes 24576

commit v3 on v2

v3 whole, which is shorter than its diff:
```python
import functools

import jax
import jax.numpy as jnp
from jax import lax
from jax.experimental import pallas as pl
from jax.experimental.pallas import tpu as pltpu
from jax.sharding import PartitionSpec as P

MESH = pl.DeviceIdType.MESH
F32 = jnp.float32
BF16 = jnp.bfloat16
HEAD_DIM = 64
STATE_DIM = 128
NYC = 8
UNITS = 48
eps = 1e-06


def rms_scale(values, norm_gain):
    squares = jnp.mean(values * values, axis=-1, keepdims=True)
    return values * lax.rsqrt(squares + eps) * norm_gain


def dot(a, b):
    return jnp.dot(a, b, preferred_element_type=F32)


def two_terms(v):
    high = v.astype(BF16).astype(F32)
    return high, (v - high).astype(BF16).astype(F32)


def dot_rows(a, b):
    return lax.dot_general(a, b, (((1,), (1,)), ((), ())), preferred_element_type=F32)


def layer_kernel(
    n_ep,
    n_tp,
    tokens_ref,
    mixer_gain_ref,
    step_weight_ref,
    step_bias_ref,
    decay_log_ref,
    skip_ref,
    inner_kernel_ref,
    state_kernel_ref,
    inner_window_ref,
    state_window_ref,
    group_gain_ref,
    gain_ref,
    routes_ref,
    route_weights_ref,
    dense_gate_ref,
    dense_up_ref,
    dense_down_ref,
    dense_scale_ref,
    gate_weight_hbm,
    inner_weight_hbm,
    state_weight_hbm,
    output_weight_hbm,
    state_hbm,
    gate_hbm,
    up_hbm,
    down_hbm,
    out_ref,
    new_inner_ref,
    new_state_window_ref,
    new_state_ref,
    gate_w,
    inner_w,
    state_w,
    output_w,
    decay_rows,
    read,
    w_gate,
    w_up,
    w_down,
    parts,
    residual_ref,
    ffn_ref,
    dw,
    dx,
    combine_ref,
    tall,
    going,
    came,
    xs,
    act,
    dz_going,
    dz_came,
    hid,
    moe_going,
    moe_came,
    tall_back,
    back_going,
    back_came,
    od_going,
    od_came,
    in_sems,
    state_sems,
    local_sems,
    send_sems,
    recv_sems,
):
    me = lax.axis_index("ep")
    t = lax.axis_index("tp")
    n_z = n_ep // NYC
    z = me // NYC
    yc = me % NYC
    seqs = tokens_ref.shape[0]
    heads = new_state_ref.shape[1]
    chunk = seqs // 4
    width = out_ref.shape[1]
    slots = 2 * n_ep

    def across_tp(k):
        return (me, lax.rem(t + k, n_tp))

    def along_z(k):
        return (lax.rem(z + k, n_z) * NYC + yc, t)

    def within_z(k):
        return (z * NYC + lax.rem(yc + k, NYC), t)

    def along_ep(kz, k):
        return (lax.rem(z + kz, n_z) * NYC + lax.rem(yc + k, NYC), t)

    steps = sorted(range(n_z), key=lambda kz: -min(kz, n_z - kz))

    def to_all(send):
        for kz in steps:
            for k in range(0 if kz else 1, NYC):
                send(along_ep(kz, k))

    def remote(src, dst, which, peer):
        return pltpu.make_async_remote_copy(
            src_ref=src,
            dst_ref=dst,
            send_sem=send_sems.at[which],
            recv_sem=recv_sems.at[which],
            device_id=peer,
            device_id_type=MESH,
        )

    def wait_in(ref, which):
        remote(ref, ref, which, across_tp(1)).wait_recv()

    def wait_out(ref, which):
        remote(ref, ref, which, across_tp(1)).wait_send()

    PART, DW, DW2, DX, OUT, DZ, HID, MOE, BACK, OD = range(10)

    mixer_loads = [
        pltpu.make_async_copy(src, dst, in_sems.at[i])
        for i, (src, dst) in enumerate(
            [
                (inner_weight_hbm, inner_w),
                (state_weight_hbm, state_w),
                (gate_weight_hbm, gate_w),
                (output_weight_hbm, output_w),
            ]
        )
    ]
    for load in mixer_loads[:3]:
        load.start()
    state_loads = [
        pltpu.make_async_copy(
            state_hbm.at[pl.ds(c * chunk, chunk)], new_state_ref.at[pl.ds(c * chunk, chunk)], state_sems.at[c]
        )
        for c in range(4)
    ]
    for load in state_loads:
        load.start()
    mixer_loads[3].start()


    barrier = pltpu.get_barrier_semaphore()
    for k in range(1, n_tp):
        pl.semaphore_signal(barrier, inc=1, device_id=across_tp(k), device_id_type=MESH)

    to_all(
        lambda peer: pl.semaphore_signal(barrier, inc=1, device_id=peer, device_id_type=MESH)
    )

    loads = [
        pltpu.make_async_copy(src.at[0], dst, local_sems.at[i])
        for i, (src, dst) in enumerate([(gate_hbm, w_gate), (up_hbm, w_up), (down_hbm, w_down)])
    ]
    for load in loads:
        load.start()

    units = dense_gate_ref.shape[0]
    gap = jnp.zeros((UNITS - units, width), F32)
    for i, ref in enumerate((dense_gate_ref, dense_up_ref, dense_down_ref)):
        dw[yc, i * UNITS : (i + 1) * UNITS] = jnp.concatenate(
            [ref[...].astype(F32), gap], axis=0
        ).astype(BF16)

    expert = lax.broadcasted_iota(jnp.int32, (n_ep, seqs), 0)
    named = [(routes_ref[k : k + 1, :] == expert).astype(F32) for k in range(2)]
    earlier = (
        lax.broadcasted_iota(jnp.int32, (seqs, seqs), 0)
        < lax.broadcasted_iota(jnp.int32, (seqs, seqs), 1)
    ).astype(F32)
    before = dot(named[0] + named[1], earlier)
    place = lax.broadcasted_iota(jnp.int32, (slots, seqs), 0)
    chosen = []
    for k in range(2):
        slot = jnp.sum(before * named[k], axis=0, keepdims=True).astype(jnp.int32)
        chosen.append((place == routes_ref[k : k + 1, :] * 2 + slot).astype(F32))
    selection = (chosen[0] + chosen[1]).astype(BF16)
    combine_ref[...] = jnp.transpose(
        chosen[0] * route_weights_ref[0:1, :] + chosen[1] * route_weights_ref[1:2, :]
    )

    normed = rms_scale(tokens_ref[...].astype(F32), mixer_gain_ref[...]).astype(BF16)
    step_raw = dot_rows(normed, step_weight_ref[...])
    step_in = step_raw + step_bias_ref[...]
    step = jnp.maximum(step_in, 0.0) + jnp.log1p(jnp.exp(-jnp.abs(step_in)))
    decay = jnp.exp(-step * jnp.exp(decay_log_ref[...]))

    mixer_loads[0].wait()
    inner_pre = dot(normed, inner_w[...]).astype(BF16).astype(F32)
    kern = inner_kernel_ref[...]
    conv = inner_pre * kern[3:4]
    for j in range(3):
        conv = conv + inner_window_ref[j].astype(F32) * kern[j : j + 1]
    inner = jax.nn.silu(conv)
    new_inner_ref[0:2] = inner_window_ref[1:3]
    new_inner_ref[2] = inner_pre.astype(BF16)

    mixer_loads[1].wait()
    vectors = []
    pres = []
    for r in range(2):
        pre = dot(normed, state_w[r]).astype(BF16).astype(F32)
        conv = pre * state_kernel_ref[3, r : r + 1, :]
        for j in range(3):
            conv = conv + state_window_ref[:, j, r, :].astype(F32) * state_kernel_ref[j, r : r + 1, :]
        vectors.append(jax.nn.silu(conv))
        pres.append(pre)
    new_state_window_ref[:, 0:2] = state_window_ref[:, 1:3]
    new_state_window_ref[:, 2] = jnp.concatenate(
        [pres[0][:, None, :], pres[1][:, None, :]], axis=1
    ).astype(BF16)
    in_vector, out_vector = vectors

    mixer_loads[2].wait()
    gate_pre = dot(normed, gate_w[...])

    lane = lax.broadcasted_iota(jnp.int32, inner.shape, 1) // HEAD_DIM
    step_wide = jnp.broadcast_to(step[:, 0:1], inner.shape)
    skip_wide = jnp.broadcast_to(skip_ref[:, 0:1], inner.shape)
    for h in range(1, heads):
        step_wide = jnp.where(lane == h, step[:, h : h + 1], step_wide)
        skip_wide = jnp.where(lane == h, skip_ref[:, h : h + 1], skip_wide)
    for h in range(heads):
        decay_rows[:, h * STATE_DIM : (h + 1) * STATE_DIM] = jnp.broadcast_to(
            decay[:, h : h + 1], (seqs, STATE_DIM)
        )
    spare = jnp.zeros((32 - seqs, inner.shape[1]), F32)
    high, low = two_terms(jnp.concatenate([step_wide * inner, spare], axis=0))
    written = jnp.transpose(
        jnp.concatenate([high, high, low, jnp.zeros_like(low)], axis=0)
    ).astype(BF16)
    spare = spare[:, :STATE_DIM]
    high, low = two_terms(jnp.concatenate([in_vector, spare], axis=0))
    inputs = jnp.concatenate([high, low, high, jnp.zeros_like(low)], axis=0)
    owner = lax.broadcasted_iota(jnp.int32, inputs.shape, 0) % 32
    high, low = two_terms(jnp.concatenate([out_vector, spare], axis=0))
    reader = jnp.concatenate([high, low, jnp.zeros((64, STATE_DIM), F32)], axis=0).astype(BF16)
    reader = jnp.concatenate([reader, reader], axis=1)
    column = lax.broadcasted_iota(jnp.int32, (heads * HEAD_DIM, STATE_DIM), 1) % 32

    for k in range(4):
        state_loads[k].wait()

        def update(i, carry):
            b = k * chunk + i
            added = dot(written, jnp.where(owner == b, inputs, 0.0).astype(BF16))
            rates = decay_rows[pl.ds(b, 1), :]
            news = []
            for h in range(heads):
                new = new_state_ref[b, h] * rates[:, h * STATE_DIM : (h + 1) * STATE_DIM] + (
                    added[h * HEAD_DIM : (h + 1) * HEAD_DIM]
                )
                new_state_ref[b, h] = new
                news.append(new)
            new = jnp.concatenate(news, axis=0)
            high = new.astype(BF16)
            both = jnp.concatenate([high, (new - high.astype(F32)).astype(BF16)], axis=1)
            read[...] = jnp.where(column == b, dot_rows(both, reader), read[...])
            return carry

        lax.fori_loop(0, chunk, update, 0, unroll=True)
    mixed = jnp.transpose(read[...])
    mixed_rows = mixed[:seqs] + mixed[32 : 32 + seqs]
    mixed_rows = mixed_rows + skip_wide * inner
    gated = mixed_rows * jax.nn.silu(gate_pre)
    mixer_rows = (rms_scale(gated, 1.0) * group_gain_ref[...]).astype(BF16)
    mixer_loads[3].wait()
    parts[t] = dot(mixer_rows, output_w[...]).astype(BF16)

    pl.semaphore_wait(barrier, n_tp - 1 + n_ep - 1)

    for k in range(1, n_tp):
        remote(parts.at[t], parts.at[t], PART, across_tp(k)).start()

    for k in range(2, NYC, 2):
        remote(dw.at[yc], dw.at[yc], DW, within_z(k)).start()

    wait_in(parts.at[pl.ds(0, n_tp - 1)], PART)
    total = parts[0].astype(F32)
    for k in range(1, n_tp):
        total = total + parts[k].astype(F32)
    residual = tokens_ref[...].astype(F32) + total
    residual_ref[...] = residual
    ffn = rms_scale(residual, gain_ref[...]).astype(BF16)
    ffn_ref[...] = ffn

    own = pl.ds(pl.multiple_of(t * width, width), width)
    dx[z] = ffn_ref[:, own]

    for k in steps[:-1]:
        remote(dx.at[z], dx.at[z], DX, along_z(k)).start()

    outgoing = dot(selection, ffn)
    lines = outgoing.shape[1] // 128
    for j in range(lines):
        tall[pl.ds(j, slots, stride=lines), :] = outgoing[:, j * 128 : (j + 1) * 128]
    going[...] = tall[...].reshape(going.shape).astype(BF16)

    to_all(lambda peer: remote(going.at[peer[0]], came.at[me], OUT, peer).start())
    came[me] = going[me]

    wait_in(dw.at[pl.ds(0, NYC // 2 - 1)], DW)
    sibling = (z * NYC + yc + 1 - 2 * lax.rem(yc, 2), t)
    for k in range(0, NYC, 2):
        held = lax.rem(yc + k, NYC)
        remote(dw.at[held], dw.at[held], DW2, sibling).start()
    wait_in(dw.at[pl.ds(0, NYC // 2)], DW2)
    wait_in(dx.at[pl.ds(0, n_z - 1)], DX)
    dense_rows = dx[...].reshape(n_z * seqs, width)
    for i in range(2):
        weights = dw[:, i * UNITS : (i + 1) * UNITS].reshape(NYC * UNITS, width)
        dz_going[:, :, i * NYC * UNITS : (i + 1) * NYC * UNITS] = (
            dot_rows(dense_rows, weights).astype(BF16).reshape(n_tp, -1, NYC * UNITS)
        )
    for k in range(1, n_tp):
        peer = across_tp(k)
        remote(dz_going.at[peer[1]], dz_came.at[t], DZ, peer).start()
    dz_came[t] = dz_going[t]

    wait_in(came.at[pl.ds(0, n_ep - 1)], OUT)
    wait_in(dz_came.at[pl.ds(0, n_tp - 1)], DZ)
    gate_up = dz_came[0].astype(F32)
    for k in range(1, n_tp):
        gate_up = gate_up + dz_came[k].astype(F32)
    hid[t] = (
        jax.nn.silu(gate_up[:, : NYC * UNITS]) * gate_up[:, NYC * UNITS :]
    ).astype(BF16)
    for k in range(1, n_tp):
        remote(hid.at[t], hid.at[t], HID, across_tp(k)).start()

    tall[...] = came[...].astype(F32).reshape(tall.shape)
    for j in range(lines):
        xs[:, j * 128 : (j + 1) * 128] = tall[pl.ds(j, slots, stride=lines), :].astype(BF16)
    loads[0].wait()
    loads[1].wait()
    rows = xs[...]
    act[...] = (jax.nn.silu(dot_rows(rows, w_gate[...])) * dot_rows(rows, w_up[...])).astype(BF16)
    loads[2].wait()
    for k in range(1, n_tp):
        peer = across_tp(k)
        columns = pl.ds(pl.multiple_of(peer[1] * width, width), width)
        moe_going[peer[1]] = dot(act[...], w_down[:, columns]).astype(BF16)
        remote(moe_going.at[peer[1]], moe_came.at[t], MOE, peer).start()
    moe_came[t] = dot(act[...], w_down[:, own]).astype(BF16)

    wait_in(hid.at[pl.ds(0, n_tp - 1)], HID)
    dense_part = dot(
        hid[...].reshape(n_z * seqs, NYC * UNITS),
        dw[:, 2 * UNITS : 3 * UNITS].reshape(NYC * UNITS, width),
    )
    od_going[...] = dense_part.astype(BF16).reshape(od_going.shape)

    for k in steps[:-1]:
        there = lax.rem(z + k, n_z)
        remote(od_going.at[there], od_came.at[z], OD, along_z(k)).start()
    od_came[z] = od_going[z]

    wait_in(moe_came.at[pl.ds(0, n_tp - 1)], MOE)
    rows_out = moe_came[0].astype(F32)
    for k in range(1, n_tp):
        rows_out = rows_out + moe_came[k].astype(F32)
    for j in range(width // 128):
        tall_back[pl.ds(j, slots, stride=2), :] = rows_out[:, j * 128 : (j + 1) * 128]
    back_going[...] = tall_back[...].reshape(back_going.shape).astype(BF16)

    to_all(lambda peer: remote(back_going.at[peer[0]], back_came.at[me], BACK, peer).start())
    back_came[me] = back_going[me]

    wait_in(od_came.at[pl.ds(0, n_z - 1)], OD)
    dense_out = od_came[0].astype(F32)
    for k in range(1, n_z):
        dense_out = dense_out + od_came[k].astype(F32)

    wait_in(back_came.at[pl.ds(0, n_ep - 1)], BACK)
    tall_back[...] = back_came[...].astype(F32).reshape(tall_back.shape)
    returned = [
        tall_back[pl.ds(j, slots, stride=2), :].astype(BF16) for j in range(width // 128)
    ]
    returned = jnp.concatenate(returned, axis=1).astype(F32)
    expert_out = jnp.dot(combine_ref[...], returned, precision=lax.Precision.HIGHEST)
    out_ref[...] = (
        residual_ref[:, own] + expert_out + dense_scale_ref[...] * dense_out
    ).astype(BF16)

    wait_out(parts.at[pl.ds(0, n_tp - 1)], PART)
    wait_out(dw.at[pl.ds(0, NYC // 2 - 1)], DW)
    wait_out(dw.at[pl.ds(0, NYC // 2)], DW2)
    wait_out(dx.at[pl.ds(0, n_z - 1)], DX)
    wait_out(going.at[pl.ds(0, n_ep - 1)], OUT)
    wait_out(dz_going.at[pl.ds(0, n_tp - 1)], DZ)
    wait_out(hid.at[pl.ds(0, n_tp - 1)], HID)
    wait_out(moe_going.at[pl.ds(0, n_tp - 1)], MOE)
    wait_out(back_going.at[pl.ds(0, n_ep - 1)], BACK)
    wait_out(od_going.at[pl.ds(0, n_z - 1)], OD)


def write_kernel(*refs):
    sems = refs[-1]
    copies = [pltpu.make_async_copy(refs[i], refs[4 + i], sems.at[i]) for i in (3, 0, 1, 2)]
    for copy in copies:
        copy.start()
    for copy in copies:
        copy.wait()


VMEM = pl.BlockSpec(memory_space=pltpu.VMEM)
ANY = pl.BlockSpec(memory_space=pl.ANY)


def local(
    n_ep,
    n_tp,
    tokens,
    mixer_gain,
    gate_weight,
    inner_weight,
    state_weight,
    step_weight,
    step_bias,
    decay_log,
    skip_scale,
    inner_kernel,
    state_kernel,
    inner_window,
    state_window,
    recurrent_state,
    group_gain,
    output_weight,
    channel_gain,
    routes,
    route_weights,
    expert_gate,
    expert_up,
    expert_down,
    dense_gate,
    dense_up,
    dense_down,
    dense_scale,
):
    seqs, model = tokens.shape
    width = dense_scale.shape[0]
    hidden = expert_gate.shape[2]
    n_z = n_ep // NYC
    slots = 2 * n_ep
    scratch = [
        pltpu.VMEM(gate_weight.shape, BF16),
        pltpu.VMEM(inner_weight.shape, BF16),
        pltpu.VMEM(state_weight.shape, BF16),
        pltpu.VMEM(output_weight.shape, BF16),
        pltpu.VMEM((seqs, step_bias.shape[0] * STATE_DIM), F32),
        pltpu.VMEM((width, STATE_DIM), F32),
        pltpu.VMEM((hidden, model), BF16),
        pltpu.VMEM((hidden, model), BF16),
        pltpu.VMEM((hidden, model), BF16),
        pltpu.VMEM((n_tp, seqs, model), BF16),
        pltpu.VMEM((seqs, model), F32),
        pltpu.VMEM((seqs, model), BF16),
        pltpu.VMEM((NYC, 3 * UNITS, width), BF16),
        pltpu.VMEM((n_z, seqs, width), BF16),
        pltpu.VMEM((seqs, slots), F32),
        pltpu.VMEM((slots * model // 128, 128), F32),
        pltpu.VMEM((n_ep, 2 * model // 128, 128), BF16),
        pltpu.VMEM((n_ep, 2 * model // 128, 128), BF16),
        pltpu.VMEM((slots, model), BF16),
        pltpu.VMEM((slots, hidden), BF16),
        pltpu.VMEM((n_tp, n_z * seqs // n_tp, 2 * NYC * UNITS), BF16),
        pltpu.VMEM((n_tp, n_z * seqs // n_tp, 2 * NYC * UNITS), BF16),
        pltpu.VMEM((n_tp, n_z * seqs // n_tp, NYC * UNITS), BF16),
        pltpu.VMEM((n_tp, slots, width), BF16),
        pltpu.VMEM((n_tp, slots, width), BF16),
        pltpu.VMEM((slots * 2, 128), F32),
        pltpu.VMEM((n_ep, 4, 128), BF16),
        pltpu.VMEM((n_ep, 4, 128), BF16),
        pltpu.VMEM((n_z, seqs, width), BF16),
        pltpu.VMEM((n_z, seqs, width), BF16),
        pltpu.SemaphoreType.DMA((4,)),
        pltpu.SemaphoreType.DMA((4,)),
        pltpu.SemaphoreType.DMA((3,)),
        pltpu.SemaphoreType.DMA((10,)),
        pltpu.SemaphoreType.DMA((10,)),
    ]
    results = [
        ((seqs, width), BF16),
        ((3, seqs, width), BF16),
        (state_window.shape, BF16),
        (recurrent_state.shape, F32),
    ]
    held = pl.pallas_call(
        functools.partial(layer_kernel, n_ep, n_tp),
        out_shape=tuple(pltpu.VMEM(*r) for r in results),
        in_specs=[VMEM] * 18 + [ANY] * 8,
        out_specs=(VMEM,) * 4,
        scratch_shapes=scratch,
        compiler_params=pltpu.CompilerParams(collective_id=0, has_side_effects=True),
        name="layer",
    )(
        tokens,
        mixer_gain[None],
        step_weight.T,
        step_bias[None],
        decay_log[None],
        skip_scale[None],
        inner_kernel,
        state_kernel,
        jnp.swapaxes(inner_window, 0, 1),
        state_window,
        group_gain[None],
        channel_gain[None],
        routes.T,
        route_weights.T,
        dense_gate.T,
        dense_up.T,
        dense_down,
        dense_scale[None],
        gate_weight,
        inner_weight,
        state_weight,
        output_weight,
        recurrent_state,
        jnp.swapaxes(expert_gate, 1, 2),
        jnp.swapaxes(expert_up, 1, 2),
        expert_down,
    )
    new_tokens, new_inner, new_window, new_state = pl.pallas_call(
        write_kernel,
        out_shape=tuple(jax.ShapeDtypeStruct(*r) for r in results),
        in_specs=[VMEM] * 4,
        out_specs=(ANY,) * 4,
        scratch_shapes=[pltpu.SemaphoreType.DMA((4,))],
        name="write",
    )(*(pltpu.with_memory_space_constraint(h, pltpu.VMEM) for h in held))
    return new_tokens, new_state, jnp.swapaxes(new_inner, 0, 1), new_window


def solution(mesh):
    placed = (
        P("ep", None),
        P(),
        P(None, "tp"),
        P(None, "tp"),
        P(None, None, "tp"),
        P(None, "tp"),
        P("tp"),
        P("tp"),
        P("tp"),
        P(None, "tp"),
        P(None, None, "tp"),
        P("ep", None, "tp"),
        P("ep", None, None, "tp"),
        P("ep", "tp", None, None),
        P("tp"),
        P("tp", None),
        P(),
        P("ep", None),
        P("ep", None),
        P("ep", None, "tp"),
        P("ep", None, "tp"),
        P("ep", "tp", None),
        P("tp", "ep"),
        P("tp", "ep"),
        P("ep", "tp"),
        P("tp"),
    )
    return jax.shard_map(
        functools.partial(local, mesh.shape["ep"], mesh.shape["tp"]),
        mesh=mesh,
        in_specs=placed,
        out_specs=(
            P("ep", "tp"),
            P("ep", "tp", None, None),
            P("ep", None, "tp"),
            P("ep", None, None, "tp"),
        ),
        check_vma=False,
    )
```

time: 53.8 us -> 45.3 us (0.84)
  Pallas kernels: 51.6 us -> 44.5 us
  local copies, waits for them, and re-layouts: 1.31 us -> 0 us
    pallas_call x2, Pallas kernels: 51.6 us -> 44.5 us  [the longest x1 42.8 us: local(): pl.pallas_call(functools.partial(layer_kernel, n_ep, n_tp), out_shape=tup...]
    unnamed x1 -> x0, local copies, waits for them, and re-layouts: 1.31 us -> none
where the time goes in v3:
time: 45.3 us; the launch traced here: 45.2 us
  Pallas kernels  44.5 us (98%)
  between operations  0.65 us (1%)
    pallas_call x1, Pallas kernels, local(): pl.pallas_call(functools.partial(layer_kernel, n_ep, n_tp), out_shape=tup...  42.8 us
    pallas_call x1, Pallas kernels, local(): pl.pallas_call(write_kernel, out_shape=tuple((jax.ShapeDtypeStruct(*r) fo...  1.71 us

profile of v3, /device:TPU:1, one launch (start us, length us, event | category | flops | bytes accessed | tf_op | source)
XLA Modules:
  0.0 45.2 jit_solution(17376451624710576636)
XLA Ops:
  0.6 42.8 %layer.1 = (bf16[24,256]{1,0:T(8,128)(2,1)S(1)}, bf16[3,24,256]{2,1,0:T(8,128)(2,1)S(1)}, bf16[24,3,2,128]{3,2,1,0:T(2,128)(2,1)S(1)}, f32[24,4,64,128]{3,2,1,0:T(8,128)S(1)}) custom-call(bf16[24,1024]{1,0:T(8,128)(2,1)} %tokens_ref.1, f32[1,1024]{1,0:T(1,128)} %bitcast.22, bf16[4,1024]{1,0:T(4,128)(2,1)} %bitcast.21, f32[1,4]{1,0:T(1,128)} %bitcast.28, ...), custom_call_target="tpu_custom_call" | custom-call | tf_op jit(solution)/shard_map/layer/pallas_call | solution.py:524
  43.5 1.7 %write.1 = (bf16[24,256]{1,0:T(8,128)(2,1)}, bf16[3,24,256]{2,1,0:T(8,128)(2,1)}, bf16[24,3,2,128]{3,2,1,0:T(2,128)(2,1)}, f32[24,4,64,128]{3,2,1,0:T(8,128)}) custom-call(bf16[24,256]{1,0:T(8,128)(2,1)S(1)} %get-tuple-element.12.refs_0_, bf16[3,24,256]{2,1,0:T(8,128)(2,1)S(1)} %get-tuple-element.13.refs_1_, ...), custom_call_target="tpu_custom_call" | custom-call | tf_op jit(solution)/shard_map/write/pallas_call | solution.py:560

commit v4 on v3

--- a/solution.py
+++ b/solution.py
@@ -38,24 +38,24 @@
 def layer_kernel(
     n_ep,
     n_tp,
-    tokens_ref,
-    mixer_gain_ref,
-    step_weight_ref,
-    step_bias_ref,
-    decay_log_ref,
-    skip_ref,
-    inner_kernel_ref,
-    state_kernel_ref,
-    inner_window_ref,
-    state_window_ref,
-    group_gain_ref,
-    gain_ref,
-    routes_ref,
-    route_weights_ref,
-    dense_gate_ref,
-    dense_up_ref,
-    dense_down_ref,
-    dense_scale_ref,
+    tokens_hbm,
+    mixer_gain_hbm,
+    step_weight_hbm,
+    step_bias_hbm,
+    decay_log_hbm,
+    skip_hbm,
+    inner_kernel_hbm,
+    state_kernel_hbm,
+    inner_window_hbm,
+    state_window_hbm,
+    group_gain_hbm,
+    gain_hbm,
+    routes_hbm,
+    route_weights_hbm,
+    dense_gate_hbm,
+    dense_up_hbm,
+    dense_down_hbm,
+    dense_scale_hbm,
     gate_weight_hbm,
     inner_weight_hbm,
     state_weight_hbm,
@@ -73,7 +73,7 @@
     state_w,
     output_w,
     decay_rows,
-    read,
+    terms,
     w_gate,
     w_up,
     w_down,
@@ -98,6 +98,26 @@
     back_came,
     od_going,
     od_came,
+    tokens_ref,
+    mixer_gain_ref,
+    step_weight_ref,
+    step_bias_ref,
+    decay_log_ref,
+    skip_ref,
+    inner_kernel_ref,
+    state_kernel_ref,
+    inner_window_ref,
+    state_window_ref,
+    group_gain_ref,
+    early_sems,
+    gain_ref,
+    routes_ref,
+    route_weights_ref,
+    dense_gate_ref,
+    dense_up_ref,
+    dense_down_ref,
+    dense_scale_ref,
+    late_sems,
     in_sems,
     state_sems,
     local_sems,
@@ -129,10 +149,10 @@
 
     steps = sorted(range(n_z), key=lambda kz: -min(kz, n_z - kz))
 
-    def to_all(send):
+    def to_all(send, steps=steps):
         for kz in steps:
             for k in range(0 if kz else 1, NYC):
-                send(along_ep(kz, k))
+                send(kz, along_ep(kz, k))
 
     def remote(src, dst, which, peer):
         return pltpu.make_async_remote_copy(
@@ -150,8 +170,28 @@
     def wait_out(ref, which):
         remote(ref, ref, which, across_tp(1)).wait_send()
 
-    PART, DW, DW2, DX, OUT, DZ, HID, MOE, BACK, OD = range(10)
-
+    PART, DW, DW2, DX, OUT, DZ, HID, MOE, MOE2, BACK, OD = range(11)
+
+    early_loads = [
+        pltpu.make_async_copy(src, dst, early_sems.at[i])
+        for i, (src, dst) in enumerate(
+            [
+                (tokens_hbm, tokens_ref),
+                (mixer_gain_hbm, mixer_gain_ref),
+                (step_weight_hbm, step_weight_ref),
+                (step_bias_hbm, step_bias_ref),
+                (decay_log_hbm, decay_log_ref),
+                (skip_hbm, skip_ref),
+                (inner_kernel_hbm, inner_kernel_ref),
+                (state_kernel_hbm, state_kernel_ref),
+                (inner_window_hbm, inner_window_ref),
+                (state_window_hbm, state_window_ref),
+                (group_gain_hbm, group_gain_ref),
+            ]
+        )
+    ]
+    for load in early_loads:
+        load.start()
     mixer_loads = [
         pltpu.make_async_copy(src, dst, in_sems.at[i])
         for i, (src, dst) in enumerate(
@@ -165,6 +205,15 @@
     ]
     for load in mixer_loads[:3]:
         load.start()
+
+    barrier = pltpu.get_barrier_semaphore()
+    for k in range(1, n_tp):
+        pl.semaphore_signal(barrier, inc=1, device_id=across_tp(k), device_id_type=MESH)
+
+    to_all(
+        lambda kz, peer: pl.semaphore_signal(barrier, inc=1, device_id=peer, device_id_type=MESH)
+    )
+
     state_loads = [
         pltpu.make_async_copy(
             state_hbm.at[pl.ds(c * chunk, chunk)], new_state_ref.at[pl.ds(c * chunk, chunk)], state_sems.at[c]
@@ -174,46 +223,24 @@
     for load in state_loads:
         load.start()
     mixer_loads[3].start()
-
-
-    barrier = pltpu.get_barrier_semaphore()
-    for k in range(1, n_tp):
-        pl.semaphore_signal(barrier, inc=1, device_id=across_tp(k), device_id_type=MESH)
-
-    to_all(
-        lambda peer: pl.semaphore_signal(barrier, inc=1, device_id=peer, device_id_type=MESH)
-    )
-
-    loads = [
-        pltpu.make_async_copy(src.at[0], dst, local_sems.at[i])
-        for i, (src, dst) in enumerate([(gate_hbm, w_gate), (up_hbm, w_up), (down_hbm, w_down)])
+    late_loads = [
+        pltpu.make_async_copy(src, dst, late_sems.at[i])
+        for i, (src, dst) in enumerate(
+            [
+                (gain_hbm, gain_ref),
+                (routes_hbm, routes_ref),
+                (route_weights_hbm, route_weights_ref),
+                (dense_gate_hbm, dense_gate_ref),
+                (dense_up_hbm, dense_up_ref),
+                (dense_down_hbm, dense_down_ref),
+                (dense_scale_hbm, dense_scale_ref),
+            ]
+        )
     ]
-    for load in loads:
+    for load in late_loads:
         load.start()
-
-    units = dense_gate_ref.shape[0]
-    gap = jnp.zeros((UNITS - units, width), F32)
-    for i, ref in enumerate((dense_gate_ref, dense_up_ref, dense_down_ref)):
-        dw[yc, i * UNITS : (i + 1) * UNITS] = jnp.concatenate(
-            [ref[...].astype(F32), gap], axis=0
-        ).astype(BF16)
-
-    expert = lax.broadcasted_iota(jnp.int32, (n_ep, seqs), 0)
-    named = [(routes_ref[k : k + 1, :] == expert).astype(F32) for k in range(2)]
-    earlier = (
-        lax.broadcasted_iota(jnp.int32, (seqs, seqs), 0)
-        < lax.broadcasted_iota(jnp.int32, (seqs, seqs), 1)
-    ).astype(F32)
-    before = dot(named[0] + named[1], earlier)
-    place = lax.broadcasted_iota(jnp.int32, (slots, seqs), 0)
-    chosen = []
-    for k in range(2):
-        slot = jnp.sum(before * named[k], axis=0, keepdims=True).astype(jnp.int32)
-        chosen.append((place == routes_ref[k : k + 1, :] * 2 + slot).astype(F32))
-    selection = (chosen[0] + chosen[1]).astype(BF16)
-    combine_ref[...] = jnp.transpose(
-        chosen[0] * route_weights_ref[0:1, :] + chosen[1] * route_weights_ref[1:2, :]
-    )
+    for load in early_loads:
+        load.wait()
 
     normed = rms_scale(tokens_ref[...].astype(F32), mixer_gain_ref[...]).astype(BF16)
     step_raw = dot_rows(normed, step_weight_ref[...])
@@ -221,7 +248,8 @@
     step = jnp.maximum(step_in, 0.0) + jnp.log1p(jnp.exp(-jnp.abs(step_in)))
     decay = jnp.exp(-step * jnp.exp(decay_log_ref[...]))
 
-    mixer_loads[0].wait()
+    for load in mixer_loads[:3]:
+        load.wait()
     inner_pre = dot(normed, inner_w[...]).astype(BF16).astype(F32)
     kern = inner_kernel_ref[...]
     conv = inner_pre * kern[3:4]
@@ -231,7 +259,6 @@
     new_inner_ref[0:2] = inner_window_ref[1:3]
     new_inner_ref[2] = inner_pre.astype(BF16)
 
-    mixer_loads[1].wait()
     vectors = []
     pres = []
     for r in range(2):
@@ -247,7 +274,6 @@
     ).astype(BF16)
     in_vector, out_vector = vectors
 
-    mixer_loads[2].wait()
     gate_pre = dot(normed, gate_w[...])
 
     lane = lax.broadcasted_iota(jnp.int32, inner.shape, 1) // HEAD_DIM
@@ -270,32 +296,36 @@
     inputs = jnp.concatenate([high, low, high, jnp.zeros_like(low)], axis=0)
     owner = lax.broadcasted_iota(jnp.int32, inputs.shape, 0) % 32
     high, low = two_terms(jnp.concatenate([out_vector, spare], axis=0))
-    reader = jnp.concatenate([high, low, jnp.zeros((64, STATE_DIM), F32)], axis=0).astype(BF16)
-    reader = jnp.concatenate([reader, reader], axis=1)
+    reader = jnp.transpose(
+        jnp.concatenate([high, low, jnp.zeros((64, STATE_DIM), F32)], axis=0)
+    ).astype(BF16)
+    read = jnp.zeros((width, STATE_DIM), F32)
     column = lax.broadcasted_iota(jnp.int32, (heads * HEAD_DIM, STATE_DIM), 1) % 32
 
     for k in range(4):
         state_loads[k].wait()
 
-        def update(i, carry):
-            b = k * chunk + i
-            added = dot(written, jnp.where(owner == b, inputs, 0.0).astype(BF16))
-            rates = decay_rows[pl.ds(b, 1), :]
-            news = []
-            for h in range(heads):
-                new = new_state_ref[b, h] * rates[:, h * STATE_DIM : (h + 1) * STATE_DIM] + (
-                    added[h * HEAD_DIM : (h + 1) * HEAD_DIM]
-                )
-                new_state_ref[b, h] = new
-                news.append(new)
-            new = jnp.concatenate(news, axis=0)
-            high = new.astype(BF16)
-            both = jnp.concatenate([high, (new - high.astype(F32)).astype(BF16)], axis=1)
-            read[...] = jnp.where(column == b, dot_rows(both, reader), read[...])
-            return carry
-
-        lax.fori_loop(0, chunk, update, 0, unroll=True)
-    mixed = jnp.transpose(read[...])
+        for i in range(chunk // 2):
+            pair = [k * chunk + 2 * i, k * chunk + 2 * i + 1]
+            added = dot(
+                written,
+                jnp.concatenate([jnp.where(owner == b, inputs, 0.0) for b in pair], axis=1).astype(BF16),
+            )
+            for n, b in enumerate(pair):
+                rates = decay_rows[pl.ds(b, 1), :]
+                news = []
+                for h in range(heads):
+                    new = new_state_ref[b, h] * rates[:, h * STATE_DIM : (h + 1) * STATE_DIM] + (
+                        added[h * HEAD_DIM : (h + 1) * HEAD_DIM, n * STATE_DIM : (n + 1) * STATE_DIM]
+                    )
+                    new_state_ref[b, h] = new
+                    news.append(new)
+                at = (2 * i + n) * width
+                terms[at : at + width] = jnp.concatenate(news, axis=0).astype(BF16)
+        found = dot(terms[...], reader)
+        for i in range(chunk):
+            read = jnp.where(column == k * chunk + i, found[i * width : (i + 1) * width], read)
+    mixed = jnp.transpose(read)
     mixed_rows = mixed[:seqs] + mixed[32 : 32 + seqs]
     mixed_rows = mixed_rows + skip_wide * inner
     gated = mixed_rows * jax.nn.silu(gate_pre)
@@ -308,8 +338,41 @@
     for k in range(1, n_tp):
         remote(parts.at[t], parts.at[t], PART, across_tp(k)).start()
 
+    for load in late_loads:
+        load.wait()
+    units = dense_gate_ref.shape[0]
+    gap = jnp.zeros((UNITS - units, width), F32)
+    for i, ref in enumerate((dense_gate_ref, dense_up_ref, dense_down_ref)):
+        dw[yc, i * UNITS : (i + 1) * UNITS] = jnp.concatenate(
+            [ref[...].astype(F32), gap], axis=0
+        ).astype(BF16)
+
     for k in range(2, NYC, 2):
         remote(dw.at[yc], dw.at[yc], DW, within_z(k)).start()
+
+    expert = lax.broadcasted_iota(jnp.int32, (n_ep, seqs), 0)
+    named = [(routes_ref[k : k + 1, :] == expert).astype(F32) for k in range(2)]
+    earlier = (
+        lax.broadcasted_iota(jnp.int32, (seqs, seqs), 0)
+        < lax.broadcasted_iota(jnp.int32, (seqs, seqs), 1)
+    ).astype(F32)
+    before = dot(named[0] + named[1], earlier)
+    place = lax.broadcasted_iota(jnp.int32, (slots, seqs), 0)
+    chosen = []
+    for k in range(2):
+        slot = jnp.sum(before * named[k], axis=0, keepdims=True).astype(jnp.int32)
+        chosen.append((place == routes_ref[k : k + 1, :] * 2 + slot).astype(F32))
+    selection = (chosen[0] + chosen[1]).astype(BF16)
+    combine_ref[...] = jnp.transpose(
+        chosen[0] * route_weights_ref[0:1, :] + chosen[1] * route_weights_ref[1:2, :]
+    )
+
+    loads = [
+        pltpu.make_async_copy(src.at[0], dst, local_sems.at[i])
+        for i, (src, dst) in enumerate([(gate_hbm, w_gate), (up_hbm, w_up), (down_hbm, w_down)])
+    ]
+    for load in loads:
+        load.start()
 
     wait_in(parts.at[pl.ds(0, n_tp - 1)], PART)
     total = parts[0].astype(F32)
@@ -332,8 +395,12 @@
         tall[pl.ds(j, slots, stride=lines), :] = outgoing[:, j * 128 : (j + 1) * 128]
     going[...] = tall[...].reshape(going.shape).astype(BF16)
 
-    to_all(lambda peer: remote(going.at[peer[0]], came.at[me], OUT, peer).start())
-    came[me] = going[me]
+    def dispatch(kz, peer):
+        place = steps.index((n_z - kz) % n_z) * NYC + yc
+        remote(going.at[peer[0]], came.at[place], OUT, peer).start()
+
+    to_all(dispatch)
+    came[(n_z - 1) * NYC + yc] = going[me]
 
     wait_in(dw.at[pl.ds(0, NYC // 2 - 1)], DW)
     sibling = (z * NYC + yc + 1 - 2 * lax.rem(yc, 2), t)
@@ -372,11 +439,17 @@
     rows = xs[...]
     act[...] = (jax.nn.silu(dot_rows(rows, w_gate[...])) * dot_rows(rows, w_up[...])).astype(BF16)
     loads[2].wait()
+    halves = [pl.ds(0, n_ep), pl.ds(n_ep, n_ep)]
     for k in range(1, n_tp):
         peer = across_tp(k)
         columns = pl.ds(pl.multiple_of(peer[1] * width, width), width)
         moe_going[peer[1]] = dot(act[...], w_down[:, columns]).astype(BF16)
-        remote(moe_going.at[peer[1]], moe_came.at[t], MOE, peer).start()
+        half = (peer[1], halves[0])
+        remote(moe_going.at[half], moe_came.at[t, halves[0]], MOE, peer).start()
+    for k in range(1, n_tp):
+        peer = across_tp(k)
+        half = (peer[1], halves[1])
+        remote(moe_going.at[half], moe_came.at[t, halves[1]], MOE2, peer).start()
     moe_came[t] = dot(act[...], w_down[:, own]).astype(BF16)
 
     wait_in(hid.at[pl.ds(0, n_tp - 1)], HID)
@@ -391,16 +464,24 @@
         remote(od_going.at[there], od_came.at[z], OD, along_z(k)).start()
     od_came[z] = od_going[z]
 
-    wait_in(moe_came.at[pl.ds(0, n_tp - 1)], MOE)
-    rows_out = moe_came[0].astype(F32)
-    for k in range(1, n_tp):
-        rows_out = rows_out + moe_came[k].astype(F32)
-    for j in range(width // 128):
-        tall_back[pl.ds(j, slots, stride=2), :] = rows_out[:, j * 128 : (j + 1) * 128]
-    back_going[...] = tall_back[...].reshape(back_going.shape).astype(BF16)
-
-    to_all(lambda peer: remote(back_going.at[peer[0]], back_came.at[me], BACK, peer).start())
-    back_came[me] = back_going[me]
+    for n, which in enumerate((MOE, MOE2)):
+        wait_in(moe_came.at[pl.ds(0, n_tp - 1), halves[n]], which)
+        rows_out = moe_came[0, halves[n]].astype(F32)
+        for k in range(1, n_tp):
+            rows_out = rows_out + moe_came[k, halves[n]].astype(F32)
+        lines = pl.ds(n * slots, slots)
+        for j in range(width // 128):
+            tall_back[pl.ds(n * slots + j, n_ep, stride=2), :] = rows_out[:, j * 128 : (j + 1) * 128]
+        back_going[pl.ds(n * n_ep // 2, n_ep // 2)] = (
+            tall_back[lines].reshape(n_ep // 2, 4, 128).astype(BF16)
+        )
+
+        def give_back(kz, peer):
+            place = steps.index(kz) * NYC + peer[0] % NYC
+            remote(back_going.at[place], back_came.at[me], BACK, peer).start()
+
+        to_all(give_back, steps[n * n_z // 2 : (n + 1) * n_z // 2])
+    back_came[me] = back_going[(n_z - 1) * NYC + yc]
 
     wait_in(od_came.at[pl.ds(0, n_z - 1)], OD)
     dense_out = od_came[0].astype(F32)
@@ -425,7 +506,8 @@
     wait_out(going.at[pl.ds(0, n_ep - 1)], OUT)
     wait_out(dz_going.at[pl.ds(0, n_tp - 1)], DZ)
     wait_out(hid.at[pl.ds(0, n_tp - 1)], HID)
-    wait_out(moe_going.at[pl.ds(0, n_tp - 1)], MOE)
+    wait_out(moe_going.at[pl.ds(0, n_tp - 1), halves[0]], MOE)
+    wait_out(moe_going.at[pl.ds(0, n_tp - 1), halves[1]], MOE2)
     wait_out(back_going.at[pl.ds(0, n_ep - 1)], BACK)
     wait_out(od_going.at[pl.ds(0, n_z - 1)], OD)
 
@@ -478,13 +560,35 @@
     hidden = expert_gate.shape[2]
     n_z = n_ep // NYC
     slots = 2 * n_ep
+    early = (
+        tokens,
+        mixer_gain[None],
+        step_weight.T,
+        step_bias[None],
+        decay_log[None],
+        skip_scale[None],
+        inner_kernel,
+        state_kernel,
+        jnp.swapaxes(inner_window, 0, 1),
+        state_window,
+        group_gain[None],
+    )
+    late = (
+        channel_gain[None],
+        routes.T,
+        route_weights.T,
+        dense_gate.T,
+        dense_up.T,
+        dense_down,
+        dense_scale[None],
+    )
     scratch = [
         pltpu.VMEM(gate_weight.shape, BF16),
         pltpu.VMEM(inner_weight.shape, BF16),
         pltpu.VMEM(state_weight.shape, BF16),
         pltpu.VMEM(output_weight.shape, BF16),
         pltpu.VMEM((seqs, step_bias.shape[0] * STATE_DIM), F32),
-        pltpu.VMEM((width, STATE_DIM), F32),
+        pltpu.VMEM((seqs // 4 * width, STATE_DIM), BF16),
         pltpu.VMEM((hidden, model), BF16),
         pltpu.VMEM((hidden, model), BF16),
         pltpu.VMEM((hidden, model), BF16),
@@ -509,11 +613,15 @@
         pltpu.VMEM((n_ep, 4, 128), BF16),
         pltpu.VMEM((n_z, seqs, width), BF16),
         pltpu.VMEM((n_z, seqs, width), BF16),
+        *[pltpu.VMEM(x.shape, x.dtype) for x in early],
+        pltpu.SemaphoreType.DMA((len(early),)),
+        *[pltpu.VMEM(x.shape, x.dtype) for x in late],
+        pltpu.SemaphoreType.DMA((len(late),)),
         pltpu.SemaphoreType.DMA((4,)),
         pltpu.SemaphoreType.DMA((4,)),
         pltpu.SemaphoreType.DMA((3,)),
-        pltpu.SemaphoreType.DMA((10,)),
-        pltpu.SemaphoreType.DMA((10,)),
+        pltpu.SemaphoreType.DMA((11,)),
+        pltpu.SemaphoreType.DMA((11,)),
     ]
     results = [
         ((seqs, width), BF16),
@@ -524,30 +632,14 @@
     held = pl.pallas_call(
         functools.partial(layer_kernel, n_ep, n_tp),
         out_shape=tuple(pltpu.VMEM(*r) for r in results),
-        in_specs=[VMEM] * 18 + [ANY] * 8,
+        in_specs=[ANY] * 26,
         out_specs=(VMEM,) * 4,
         scratch_shapes=scratch,
         compiler_params=pltpu.CompilerParams(collective_id=0, has_side_effects=True),
         name="layer",
     )(
-        tokens,
-        mixer_gain[None],
-        step_weight.T,
-        step_bias[None],
-        decay_log[None],
-        skip_scale[None],
-        inner_kernel,
-        state_kernel,
-        jnp.swapaxes(inner_window, 0, 1),
-        state_window,
-        group_gain[None],
-        channel_gain[None],
-        routes.T,
-        route_weights.T,
-        dense_gate.T,
-        dense_up.T,
-        dense_down,
-        dense_scale[None],
+        *early,
+        *late,
         gate_weight,
         inner_weight,
         state_weight,

time: 45.3 us -> 43.2 us (0.954)
  Pallas kernels: 44.5 us -> 42.5 us
    pallas_call x1, Pallas kernels: 42.8 us -> 40.8 us  [local(): pl.pallas_call(functools.partial(layer_kernel, n_ep, n_tp), out_shape=tup...]
where the time goes in v4:
time: 43.2 us
  Pallas kernels  42.5 us (98%)
  between operations  0.65 us (2%)
    pallas_call x1, Pallas kernels, local(): pl.pallas_call(functools.partial(layer_kernel, n_ep, n_tp), out_shape=tup...  40.8 us
    pallas_call x1, Pallas kernels, local(): pl.pallas_call(write_kernel, out_shape=tuple((jax.ShapeDtypeStruct(*r) fo...  1.71 us

profile of v4, /device:TPU:1, one launch (start us, length us, event | category | flops | bytes accessed | tf_op | source)
XLA Modules:
  0.0 43.2 jit_solution(13904019160116293705)
XLA Ops:
  0.6 40.8 %layer.1 = (bf16[24,256]{1,0:T(8,128)(2,1)S(1)}, bf16[3,24,256]{2,1,0:T(8,128)(2,1)S(1)}, bf16[24,3,2,128]{3,2,1,0:T(2,128)(2,1)S(1)}, f32[24,4,64,128]{3,2,1,0:T(8,128)S(1)}) custom-call(bf16[24,1024]{1,0:T(8,128)(2,1)} %tokens_hbm.1, f32[1,1024]{1,0:T(1,128)} %bitcast.22, bf16[4,1024]{1,0:T(4,128)(2,1)} %bitcast.21, f32[1,4]{1,0:T(1,128)} %bitcast.28, ...), custom_call_target="tpu_custom_call" | custom-call | tf_op jit(solution)/shard_map/layer/pallas_call | solution.py:632
  41.4 1.7 %write.1 = (bf16[24,256]{1,0:T(8,128)(2,1)}, bf16[3,24,256]{2,1,0:T(8,128)(2,1)}, bf16[24,3,2,128]{3,2,1,0:T(2,128)(2,1)}, f32[24,4,64,128]{3,2,1,0:T(8,128)}) custom-call(bf16[24,256]{1,0:T(8,128)(2,1)S(1)} %get-tuple-element.12.refs_0_, bf16[3,24,256]{2,1,0:T(8,128)(2,1)S(1)} %get-tuple-element.13.refs_1_, ...), custom_call_target="tpu_custom_call" | custom-call | tf_op jit(solution)/shard_map/write/pallas_call | solution.py:652

commit v5 on v4

--- a/solution.py
+++ b/solution.py
@@ -73,7 +73,6 @@
     state_w,
     output_w,
     decay_rows,
-    terms,
     w_gate,
     w_up,
     w_down,
@@ -123,6 +122,7 @@
     local_sems,
     send_sems,
     recv_sems,
+    rounds,
 ):
     me = lax.axis_index("ep")
     t = lax.axis_index("tp")
@@ -210,9 +210,10 @@
     for k in range(1, n_tp):
         pl.semaphore_signal(barrier, inc=1, device_id=across_tp(k), device_id_type=MESH)
 
-    to_all(
-        lambda kz, peer: pl.semaphore_signal(barrier, inc=1, device_id=peer, device_id_type=MESH)
-    )
+    for k in range(1, NYC):
+        pl.semaphore_signal(barrier, inc=1, device_id=within_z(k), device_id_type=MESH)
+    for k in (1, n_z - 1):
+        pl.semaphore_signal(barrier, inc=1, device_id=along_z(k), device_id_type=MESH)
 
     state_loads = [
         pltpu.make_async_copy(
@@ -277,63 +278,45 @@
     gate_pre = dot(normed, gate_w[...])
 
     lane = lax.broadcasted_iota(jnp.int32, inner.shape, 1) // HEAD_DIM
-    step_wide = jnp.broadcast_to(step[:, 0:1], inner.shape)
-    skip_wide = jnp.broadcast_to(skip_ref[:, 0:1], inner.shape)
-    for h in range(1, heads):
-        step_wide = jnp.where(lane == h, step[:, h : h + 1], step_wide)
-        skip_wide = jnp.where(lane == h, skip_ref[:, h : h + 1], skip_wide)
-    for h in range(heads):
-        decay_rows[:, h * STATE_DIM : (h + 1) * STATE_DIM] = jnp.broadcast_to(
-            decay[:, h : h + 1], (seqs, STATE_DIM)
-        )
-    spare = jnp.zeros((32 - seqs, inner.shape[1]), F32)
-    high, low = two_terms(jnp.concatenate([step_wide * inner, spare], axis=0))
-    written = jnp.transpose(
-        jnp.concatenate([high, high, low, jnp.zeros_like(low)], axis=0)
-    ).astype(BF16)
-    spare = spare[:, :STATE_DIM]
-    high, low = two_terms(jnp.concatenate([in_vector, spare], axis=0))
-    inputs = jnp.concatenate([high, low, high, jnp.zeros_like(low)], axis=0)
-    owner = lax.broadcasted_iota(jnp.int32, inputs.shape, 0) % 32
+
+    def widen(v):
+        wide = jnp.broadcast_to(v[:, 0:1], inner.shape)
+        for h in range(1, heads):
+            wide = jnp.where(lane == h, v[:, h : h + 1], wide)
+        return wide
+
+    spare = jnp.zeros((32 - seqs, STATE_DIM), F32)
     high, low = two_terms(jnp.concatenate([out_vector, spare], axis=0))
     reader = jnp.transpose(
         jnp.concatenate([high, low, jnp.zeros((64, STATE_DIM), F32)], axis=0)
     ).astype(BF16)
     read = jnp.zeros((width, STATE_DIM), F32)
-    column = lax.broadcasted_iota(jnp.int32, (heads * HEAD_DIM, STATE_DIM), 1) % 32
+    column = lax.broadcasted_iota(jnp.int32, (width, STATE_DIM), 1) % 32
+    written_rows = widen(step) * inner
+    fresh = written_rows * jnp.sum(in_vector * out_vector, axis=1, keepdims=True)
+    fresh = fresh + widen(skip_ref[...]) * inner
+    decay_wide = widen(decay)
+    opened = jax.nn.silu(gate_pre)
+
+    pl.semaphore_wait(barrier, n_tp - 1 + NYC - 1 + 2)
+    for k in (1, n_z - 1):
+        pl.semaphore_signal(rounds.at[0], inc=1, device_id=along_z(k), device_id_type=MESH)
 
     for k in range(4):
         state_loads[k].wait()
-
-        for i in range(chunk // 2):
-            pair = [k * chunk + 2 * i, k * chunk + 2 * i + 1]
-            added = dot(
-                written,
-                jnp.concatenate([jnp.where(owner == b, inputs, 0.0) for b in pair], axis=1).astype(BF16),
-            )
-            for n, b in enumerate(pair):
-                rates = decay_rows[pl.ds(b, 1), :]
-                news = []
-                for h in range(heads):
-                    new = new_state_ref[b, h] * rates[:, h * STATE_DIM : (h + 1) * STATE_DIM] + (
-                        added[h * HEAD_DIM : (h + 1) * HEAD_DIM, n * STATE_DIM : (n + 1) * STATE_DIM]
-                    )
-                    new_state_ref[b, h] = new
-                    news.append(new)
-                at = (2 * i + n) * width
-                terms[at : at + width] = jnp.concatenate(news, axis=0).astype(BF16)
-        found = dot(terms[...], reader)
+        olds = new_state_ref[k * chunk : (k + 1) * chunk].reshape(chunk * width, STATE_DIM)
+        found = dot(olds.astype(BF16), reader)
         for i in range(chunk):
             read = jnp.where(column == k * chunk + i, found[i * width : (i + 1) * width], read)
+    pl.semaphore_wait(rounds.at[0], 2)
+    for k in (2, n_z - 2):
+        pl.semaphore_signal(rounds.at[1], inc=1, device_id=along_z(k), device_id_type=MESH)
+
     mixed = jnp.transpose(read)
-    mixed_rows = mixed[:seqs] + mixed[32 : 32 + seqs]
-    mixed_rows = mixed_rows + skip_wide * inner
-    gated = mixed_rows * jax.nn.silu(gate_pre)
+    gated = (decay_wide * (mixed[:seqs] + mixed[32 : 32 + seqs]) + fresh) * opened
     mixer_rows = (rms_scale(gated, 1.0) * group_gain_ref[...]).astype(BF16)
     mixer_loads[3].wait()
     parts[t] = dot(mixer_rows, output_w[...]).astype(BF16)
-
-    pl.semaphore_wait(barrier, n_tp - 1 + n_ep - 1)
 
     for k in range(1, n_tp):
         remote(parts.at[t], parts.at[t], PART, across_tp(k)).start()
@@ -374,6 +357,36 @@
     for load in loads:
         load.start()
 
+    pl.semaphore_wait(rounds.at[1], 2)
+    for k in range(1, NYC):
+        pl.semaphore_signal(rounds.at[2], inc=1, device_id=within_z(k), device_id_type=MESH)
+
+    for h in range(heads):
+        decay_rows[:, h * STATE_DIM : (h + 1) * STATE_DIM] = jnp.broadcast_to(
+            decay[:, h : h + 1], (seqs, STATE_DIM)
+        )
+    high, low = two_terms(
+        jnp.concatenate([written_rows, jnp.zeros((32 - seqs, width), F32)], axis=0)
+    )
+    written = jnp.transpose(
+        jnp.concatenate([high, high, low, jnp.zeros_like(low)], axis=0)
+    ).astype(BF16)
+    high, low = two_terms(jnp.concatenate([in_vector, spare], axis=0))
+    inputs = jnp.concatenate([high, low, high, jnp.zeros_like(low)], axis=0)
+    owner = lax.broadcasted_iota(jnp.int32, inputs.shape, 0) % 32
+    for first in range(0, seqs, 2):
+        pair = (first, first + 1)
+        added = dot(
+            written,
+            jnp.concatenate([jnp.where(owner == b, inputs, 0.0) for b in pair], axis=1).astype(BF16),
+        )
+        for n, b in enumerate(pair):
+            rates = decay_rows[b : b + 1, :]
+            for h in range(heads):
+                new_state_ref[b, h] = new_state_ref[b, h] * rates[:, h * STATE_DIM : (h + 1) * STATE_DIM] + (
+                    added[h * HEAD_DIM : (h + 1) * HEAD_DIM, n * STATE_DIM : (n + 1) * STATE_DIM]
+                )
+
     wait_in(parts.at[pl.ds(0, n_tp - 1)], PART)
     total = parts[0].astype(F32)
     for k in range(1, n_tp):
@@ -395,6 +408,7 @@
         tall[pl.ds(j, slots, stride=lines), :] = outgoing[:, j * 128 : (j + 1) * 128]
     going[...] = tall[...].reshape(going.shape).astype(BF16)
 
+    pl.semaphore_wait(rounds.at[2], NYC - 1)
     def dispatch(kz, peer):
         place = steps.index((n_z - kz) % n_z) * NYC + yc
         remote(going.at[peer[0]], came.at[place], OUT, peer).start()
@@ -421,16 +435,6 @@
     dz_came[t] = dz_going[t]
 
     wait_in(came.at[pl.ds(0, n_ep - 1)], OUT)
-    wait_in(dz_came.at[pl.ds(0, n_tp - 1)], DZ)
-    gate_up = dz_came[0].astype(F32)
-    for k in range(1, n_tp):
-        gate_up = gate_up + dz_came[k].astype(F32)
-    hid[t] = (
-        jax.nn.silu(gate_up[:, : NYC * UNITS]) * gate_up[:, NYC * UNITS :]
-    ).astype(BF16)
-    for k in range(1, n_tp):
-        remote(hid.at[t], hid.at[t], HID, across_tp(k)).start()
-
     tall[...] = came[...].astype(F32).reshape(tall.shape)
     for j in range(lines):
         xs[:, j * 128 : (j + 1) * 128] = tall[pl.ds(j, slots, stride=lines), :].astype(BF16)
@@ -452,17 +456,15 @@
         remote(moe_going.at[half], moe_came.at[t, halves[1]], MOE2, peer).start()
     moe_came[t] = dot(act[...], w_down[:, own]).astype(BF16)
 
-    wait_in(hid.at[pl.ds(0, n_tp - 1)], HID)
-    dense_part = dot(
-        hid[...].reshape(n_z * seqs, NYC * UNITS),
-        dw[:, 2 * UNITS : 3 * UNITS].reshape(NYC * UNITS, width),
-    )
-    od_going[...] = dense_part.astype(BF16).reshape(od_going.shape)
-
-    for k in steps[:-1]:
-        there = lax.rem(z + k, n_z)
-        remote(od_going.at[there], od_came.at[z], OD, along_z(k)).start()
-    od_came[z] = od_going[z]
+    wait_in(dz_came.at[pl.ds(0, n_tp - 1)], DZ)
+    gate_up = dz_came[0].astype(F32)
+    for k in range(1, n_tp):
+        gate_up = gate_up + dz_came[k].astype(F32)
+    hid[t] = (
+        jax.nn.silu(gate_up[:, : NYC * UNITS]) * gate_up[:, NYC * UNITS :]
+    ).astype(BF16)
+    for k in range(1, n_tp):
+        remote(hid.at[t], hid.at[t], HID, across_tp(k)).start()
 
     for n, which in enumerate((MOE, MOE2)):
         wait_in(moe_came.at[pl.ds(0, n_tp - 1), halves[n]], which)
@@ -482,6 +484,18 @@
 
         to_all(give_back, steps[n * n_z // 2 : (n + 1) * n_z // 2])
     back_came[me] = back_going[(n_z - 1) * NYC + yc]
+
+    wait_in(hid.at[pl.ds(0, n_tp - 1)], HID)
+    dense_part = dot(
+        hid[...].reshape(n_z * seqs, NYC * UNITS),
+        dw[:, 2 * UNITS : 3 * UNITS].reshape(NYC * UNITS, width),
+    )
+    od_going[...] = dense_part.astype(BF16).reshape(od_going.shape)
+
+    for k in steps[:-1]:
+        there = lax.rem(z + k, n_z)
+        remote(od_going.at[there], od_came.at[z], OD, along_z(k)).start()
+    od_came[z] = od_going[z]
 
     wait_in(od_came.at[pl.ds(0, n_z - 1)], OD)
     dense_out = od_came[0].astype(F32)
@@ -588,7 +602,6 @@
         pltpu.VMEM(state_weight.shape, BF16),
         pltpu.VMEM(output_weight.shape, BF16),
         pltpu.VMEM((seqs, step_bias.shape[0] * STATE_DIM), F32),
-        pltpu.VMEM((seqs // 4 * width, STATE_DIM), BF16),
         pltpu.VMEM((hidden, model), BF16),
         pltpu.VMEM((hidden, model), BF16),
         pltpu.VMEM((hidden, model), BF16),
@@ -622,6 +635,7 @@
         pltpu.SemaphoreType.DMA((3,)),
         pltpu.SemaphoreType.DMA((11,)),
         pltpu.SemaphoreType.DMA((11,)),
+        pltpu.SemaphoreType.REGULAR((3,)),
     ]
     results = [
         ((seqs, width), BF16),

time: 43.2 us -> 41.8 us (0.968)
  Pallas kernels: 42.5 us -> 41.1 us
    pallas_call x1, Pallas kernels: 40.8 us -> 39.3 us  [local(): pl.pallas_call(functools.partial(layer_kernel, n_ep, n_tp), out_shape=tup...]
where the time goes in v5:
time: 41.8 us; the launch traced here: 41.7 us
  Pallas kernels  41.1 us (98%)
  between operations  0.65 us (2%)
    pallas_call x1, Pallas kernels, local(): pl.pallas_call(functools.partial(layer_kernel, n_ep, n_tp), out_shape=tup...  39.3 us
    pallas_call x1, Pallas kernels, local(): pl.pallas_call(write_kernel, out_shape=tuple((jax.ShapeDtypeStruct(*r) fo...  1.71 us

profile of v5, /device:TPU:1, one launch (start us, length us, event | category | flops | bytes accessed | tf_op | source)
XLA Modules:
  0.0 41.7 jit_solution(16934494602538805505)
XLA Ops:
  0.6 39.3 %layer.1 = (bf16[24,256]{1,0:T(8,128)(2,1)S(1)}, bf16[3,24,256]{2,1,0:T(8,128)(2,1)S(1)}, bf16[24,3,2,128]{3,2,1,0:T(2,128)(2,1)S(1)}, f32[24,4,64,128]{3,2,1,0:T(8,128)S(1)}) custom-call(bf16[24,1024]{1,0:T(8,128)(2,1)} %tokens_hbm.1, f32[1,1024]{1,0:T(1,128)} %bitcast.22, bf16[4,1024]{1,0:T(4,128)(2,1)} %bitcast.21, f32[1,4]{1,0:T(1,128)} %bitcast.28, ...), custom_call_target="tpu_custom_call" | custom-call | tf_op jit(solution)/shard_map/layer/pallas_call | solution.py:646
  40.0 1.7 %write.1 = (bf16[24,256]{1,0:T(8,128)(2,1)}, bf16[3,24,256]{2,1,0:T(8,128)(2,1)}, bf16[24,3,2,128]{3,2,1,0:T(2,128)(2,1)}, f32[24,4,64,128]{3,2,1,0:T(8,128)}) custom-call(bf16[24,256]{1,0:T(8,128)(2,1)S(1)} %get-tuple-element.12.refs_0_, bf16[3,24,256]{2,1,0:T(8,128)(2,1)S(1)} %get-tuple-element.13.refs_1_, ...), custom_call_target="tpu_custom_call" | custom-call | tf_op jit(solution)/shard_map/write/pallas_call | solution.py:666

commit v6 on v5

--- a/solution.py
+++ b/solution.py
@@ -13,6 +13,7 @@
 HEAD_DIM = 64
 STATE_DIM = 128
 NYC = 8
+STATE_CHUNKS = 2
 UNITS = 48
 eps = 1e-06
 
@@ -131,7 +132,7 @@
     yc = me % NYC
     seqs = tokens_ref.shape[0]
     heads = new_state_ref.shape[1]
-    chunk = seqs // 4
+    chunk = seqs // STATE_CHUNKS
     width = out_ref.shape[1]
     slots = 2 * n_ep
 
@@ -219,7 +220,7 @@
         pltpu.make_async_copy(
             state_hbm.at[pl.ds(c * chunk, chunk)], new_state_ref.at[pl.ds(c * chunk, chunk)], state_sems.at[c]
         )
-        for c in range(4)
+        for c in range(STATE_CHUNKS)
     ]
     for load in state_loads:
         load.start()
@@ -240,10 +241,12 @@
     ]
     for load in late_loads:
         load.start()
-    for load in early_loads:
+    for load in early_loads[:2]:
         load.wait()
 
     normed = rms_scale(tokens_ref[...].astype(F32), mixer_gain_ref[...]).astype(BF16)
+    for load in early_loads[2:]:
+        load.wait()
     step_raw = dot_rows(normed, step_weight_ref[...])
     step_in = step_raw + step_bias_ref[...]
     step = jnp.maximum(step_in, 0.0) + jnp.log1p(jnp.exp(-jnp.abs(step_in)))
@@ -302,7 +305,7 @@
     for k in (1, n_z - 1):
         pl.semaphore_signal(rounds.at[0], inc=1, device_id=along_z(k), device_id_type=MESH)
 
-    for k in range(4):
+    for k in range(STATE_CHUNKS):
         state_loads[k].wait()
         olds = new_state_ref[k * chunk : (k + 1) * chunk].reshape(chunk * width, STATE_DIM)
         found = dot(olds.astype(BF16), reader)

time: 41.8 us -> 41.7 us (level)
  no operation moved by 1% of the time
where the time goes in v6:
time: 41.7 us; the launch traced here: 41.6 us
  Pallas kernels  40.9 us (98%)
  between operations  0.65 us (2%)
    pallas_call x1, Pallas kernels, local(): pl.pallas_call(functools.partial(layer_kernel, n_ep, n_tp), out_shape=tup...  39.2 us
    pallas_call x1, Pallas kernels, local(): pl.pallas_call(write_kernel, out_shape=tuple((jax.ShapeDtypeStruct(*r) fo...  1.71 us

profile of v6, /device:TPU:1, one launch (start us, length us, event | category | flops | bytes accessed | tf_op | source)
XLA Modules:
  0.0 41.6 jit_solution(16125764609792181347)
XLA Ops:
  0.6 39.2 %layer.1 = (bf16[24,256]{1,0:T(8,128)(2,1)S(1)}, bf16[3,24,256]{2,1,0:T(8,128)(2,1)S(1)}, bf16[24,3,2,128]{3,2,1,0:T(2,128)(2,1)S(1)}, f32[24,4,64,128]{3,2,1,0:T(8,128)S(1)}) custom-call(bf16[24,1024]{1,0:T(8,128)(2,1)} %tokens_hbm.1, f32[1,1024]{1,0:T(1,128)} %bitcast.22, bf16[4,1024]{1,0:T(4,128)(2,1)} %bitcast.21, f32[1,4]{1,0:T(1,128)} %bitcast.28, ...), custom_call_target="tpu_custom_call" | custom-call | tf_op jit(solution)/shard_map/layer/pallas_call | solution.py:649
  39.9 1.7 %write.1 = (bf16[24,256]{1,0:T(8,128)(2,1)}, bf16[3,24,256]{2,1,0:T(8,128)(2,1)}, bf16[24,3,2,128]{3,2,1,0:T(2,128)(2,1)}, f32[24,4,64,128]{3,2,1,0:T(8,128)}) custom-call(bf16[24,256]{1,0:T(8,128)(2,1)S(1)} %get-tuple-element.12.refs_0_, bf16[3,24,256]{2,1,0:T(8,128)(2,1)S(1)} %get-tuple-element.13.refs_1_, ...), custom_call_target="tpu_custom_call" | custom-call | tf_op jit(solution)/shard_map/write/pallas_call | solution.py:669

commit v7 on v6

--- a/solution.py
+++ b/solution.py
@@ -252,7 +252,7 @@
     step = jnp.maximum(step_in, 0.0) + jnp.log1p(jnp.exp(-jnp.abs(step_in)))
     decay = jnp.exp(-step * jnp.exp(decay_log_ref[...]))
 
-    for load in mixer_loads[:3]:
+    for load in mixer_loads[:2]:
         load.wait()
     inner_pre = dot(normed, inner_w[...]).astype(BF16).astype(F32)
     kern = inner_kernel_ref[...]
@@ -278,6 +278,7 @@
     ).astype(BF16)
     in_vector, out_vector = vectors
 
+    mixer_loads[2].wait()
     gate_pre = dot(normed, gate_w[...])
 
     lane = lax.broadcasted_iota(jnp.int32, inner.shape, 1) // HEAD_DIM

time: 41.7 us -> 41.7 us (level)
  no operation moved by 1% of the time
where the time goes in v7:
time: 41.7 us; the launch traced here: 41.6 us
  Pallas kernels  40.9 us (98%)
  between operations  0.65 us (2%)
    pallas_call x1, Pallas kernels, local(): pl.pallas_call(functools.partial(layer_kernel, n_ep, n_tp), out_shape=tup...  39.2 us
    pallas_call x1, Pallas kernels, local(): pl.pallas_call(write_kernel, out_shape=tuple((jax.ShapeDtypeStruct(*r) fo...  1.71 us

profile of v7, /device:TPU:1, one launch (start us, length us, event | category | flops | bytes accessed | tf_op | source)
XLA Modules:
  0.0 41.6 jit_solution(14523762263002602670)
XLA Ops:
  0.6 39.2 %layer.1 = (bf16[24,256]{1,0:T(8,128)(2,1)S(1)}, bf16[3,24,256]{2,1,0:T(8,128)(2,1)S(1)}, bf16[24,3,2,128]{3,2,1,0:T(2,128)(2,1)S(1)}, f32[24,4,64,128]{3,2,1,0:T(8,128)S(1)}) custom-call(bf16[24,1024]{1,0:T(8,128)(2,1)} %tokens_hbm.1, f32[1,1024]{1,0:T(1,128)} %bitcast.22, bf16[4,1024]{1,0:T(4,128)(2,1)} %bitcast.21, f32[1,4]{1,0:T(1,128)} %bitcast.28, ...), custom_call_target="tpu_custom_call" | custom-call | tf_op jit(solution)/shard_map/layer/pallas_call | solution.py:650
  39.9 1.7 %write.1 = (bf16[24,256]{1,0:T(8,128)(2,1)}, bf16[3,24,256]{2,1,0:T(8,128)(2,1)}, bf16[24,3,2,128]{3,2,1,0:T(2,128)(2,1)}, f32[24,4,64,128]{3,2,1,0:T(8,128)}) custom-call(bf16[24,256]{1,0:T(8,128)(2,1)S(1)} %get-tuple-element.12.refs_0_, bf16[3,24,256]{2,1,0:T(8,128)(2,1)S(1)} %get-tuple-element.13.refs_1_, ...), custom_call_target="tpu_custom_call" | custom-call | tf_op jit(solution)/shard_map/write/pallas_call | solution.py:670
